TPU v7x, 32 devices: a whole 2x2x4 slice. The times are simulated.
32 devices in a mesh: sp: 16 (over z, y, x), tp: 2 (over core).
Axes of the slice: x: 2, y: 2, z: 4, core: 2. Of those that a mesh axis runs over, the one named last changes fastest.
Arguments:
- tokens: bfloat16 [8192, 2048], P('sp', 'tp'), may hold values from -6 to 6
- norm_gain: float32 [2048], replicated, may hold values from 0.1 to 1.9
- outer_gate: bfloat16 [2048, 1024], P('sp', 'tp'), may hold values from -0.125 to 0.125
- inner_gate: bfloat16 [2048, 1024], P('sp', 'tp'), may hold values from -0.125 to 0.125
- conv_input: bfloat16 [2048, 1024], P('sp', 'tp'), may hold values from -0.125 to 0.125
- query_proj: bfloat16 [2048, 1024], P('sp', 'tp'), may hold values from -0.125 to 0.125
- key_proj: bfloat16 [2048, 1024], P('sp', 'tp'), may hold values from -0.125 to 0.125
- value_proj: bfloat16 [2048, 1024], P('sp', 'tp'), may hold values from -0.125 to 0.125
- out_gate: bfloat16 [2048, 1024], P('sp', 'tp'), may hold values from -0.125 to 0.125
- conv_taps: float32 [3, 1024], P(None, 'tp'), may hold values from -3.5 to 3.5
- log_decay: float32 [2, 16, 8192], P(None, 'tp', 'sp'), may hold values from -1.2 to 0, as said below
- head_gain: float32 [1024], P('tp'), may hold values from 0.1 to 1.9
- conv_output: bfloat16 [1024, 2048], P('tp', 'sp'), may hold values from -0.1875 to 0.1875
- retention_output: bfloat16 [1024, 2048], P('tp', 'sp'), may hold values from -0.1875 to 0.1875
Outputs:
- mixed: bfloat16 [8192, 2048], P(('sp', 'tp'))
Inputs may be any that keep to these rules, and one draw needn't show every extreme that they name: `log_decay`: logarithms of per-position decays, below zero.
All inputs are finite; a program needn't handle non-finite values.
Results may differ from a plain program's by a relative error of at most 0.02.
Values may be sent and summed in bfloat16 or wider, within the bound.
A program may use at most 128 MiB of HBM per device.

v0:
```python
import jax
import functools
import jax.numpy as jnp
import numpy as np
from jax import lax
from jax.experimental import pallas as pl
from jax.experimental.pallas import tpu as pltpu
from jax.sharding import PartitionSpec as P

HEAD_DIM = 64


EPS = 1e-06
THETA = 10000.0


def with_halo(shard, sides, width):
    for axis, dim in sides:
        size, length = (lax.axis_size(axis), shard.shape[dim])
        up = [(i, (i + 1) % size) for i in range(size - 1)]
        down = [(j, i) for i, j in up]
        last = lax.slice_in_dim(shard, length - width, length, axis=dim)
        first = lax.slice_in_dim(shard, 0, width, axis=dim)
        before = lax.ppermute(last, axis, up)
        after = lax.ppermute(first, axis, down)
        shard = jnp.concatenate([before, shard, after], axis=dim)
    return shard


def rotate(field_in, position_list):
    half_dim = field_in.shape[-1] // 2
    frequency = jnp.exp(
        -jnp.log(THETA) * jnp.arange(half_dim, dtype=jnp.float32) * (2.0 / field_in.shape[-1])
    )
    angles = position_list.astype(jnp.float32)[:, None, None] * frequency
    cosine = jnp.cos(angles)
    sine_part = jnp.sin(angles)
    leading = field_in[..., :half_dim]
    trailing = field_in[..., half_dim:]
    return jnp.concatenate(
        [leading * cosine - trailing * sine_part, leading * sine_part + trailing * cosine], axis=-1
    )


def conv_branch(outer_rows, inner_rows, conv_values, conv_taps):
    inner_value = (inner_rows.astype(jnp.float32) * conv_values.astype(jnp.float32)).astype(
        jnp.bfloat16
    )
    padded = with_halo(inner_value, (("sp", 0),), 1).astype(jnp.float32)
    convolved = conv_taps[0] * padded[:-2] + conv_taps[1] * padded[1:-1] + conv_taps[2] * padded[2:]
    return (outer_rows.astype(jnp.float32) * convolved).astype(jnp.bfloat16)


def span_parts(query_rows, key_rows, value_rows, log_rates):
    length = query_rows.shape[0]
    forward_cum = jnp.cumsum(log_rates[0], axis=-1)
    backward_cum = jnp.flip(jnp.cumsum(jnp.flip(log_rates[1], -1), axis=-1), -1)
    row_index = lax.broadcasted_iota(jnp.int32, (length, length), 0)
    col_index = lax.broadcasted_iota(jnp.int32, (length, length), 1)
    lower_part = (col_index <= row_index)[None]
    spread = jnp.where(
        lower_part,
        forward_cum[:, :, None] - forward_cum[:, None, :],
        backward_cum[:, :, None] - backward_cum[:, None, :],
    )
    scores = jnp.einsum("ihe,jhe->hij", query_rows, key_rows, preferred_element_type=jnp.float32)
    weighted = (scores * jnp.exp(spread)).astype(jnp.bfloat16)
    local_part = jnp.einsum(
        "hij,jhe->ihe", weighted, value_rows, preferred_element_type=jnp.float32
    )
    key_wide = key_rows.astype(jnp.float32)
    forward_keys = (key_wide * jnp.exp(forward_cum[:, -1:] - forward_cum).T[:, :, None]).astype(
        jnp.bfloat16
    )
    backward_keys = (key_wide * jnp.exp(backward_cum[:, :1] - backward_cum).T[:, :, None]).astype(
        jnp.bfloat16
    )
    forward_state = jnp.einsum(
        "jhd,jhe->hde", forward_keys, value_rows, preferred_element_type=jnp.float32
    )
    backward_state = jnp.einsum(
        "jhd,jhe->hde", backward_keys, value_rows, preferred_element_type=jnp.float32
    )
    return (local_part, forward_cum, backward_cum, forward_state, backward_state)


def retention_branch(query_rows, key_rows, value_rows, gate_rows, log_decay, head_gain, offsets):
    row_count = query_rows.shape[0]
    head_count = query_rows.shape[1] // HEAD_DIM
    shape_heads = (row_count, head_count, HEAD_DIM)
    rotated_query = rotate(query_rows.astype(jnp.float32).reshape(shape_heads), offsets).astype(
        jnp.bfloat16
    )
    rotated_key = (
        rotate(key_rows.astype(jnp.float32).reshape(shape_heads), offsets) * HEAD_DIM ** (-0.5)
    ).astype(jnp.bfloat16)
    local_part, forward_cum, backward_cum, forward_state, backward_state = span_parts(
        rotated_query, rotated_key, value_rows.reshape(shape_heads), log_decay
    )
    forward_total = forward_cum[:, -1]
    backward_total = backward_cum[:, 0]
    totals = lax.all_gather(
        jnp.stack([forward_total, backward_total])[None], "sp", axis=0, tiled=True
    )
    inclusive = jnp.cumsum(totals, axis=0)
    exclusive = inclusive - totals
    own_index = lax.axis_index("sp")
    own_inclusive = lax.dynamic_index_in_dim(inclusive, own_index, 0, keepdims=False)
    own_exclusive = lax.dynamic_index_in_dim(exclusive, own_index, 0, keepdims=False)
    pieces = (
        lax.all_gather(forward_state[None], "sp", axis=0, tiled=True),
        lax.all_gather(backward_state[None], "sp", axis=0, tiled=True),
    )
    piece_count = pieces[0].shape[0]
    span_index = lax.iota(jnp.int32, piece_count)
    forward_weight = jnp.where(
        (span_index < own_index)[:, None],
        jnp.exp(jnp.minimum(own_exclusive[0] - inclusive[:, 0], 0.0)),
        0.0,
    )
    backward_weight = jnp.where(
        (span_index > own_index)[:, None],
        jnp.exp(jnp.minimum(exclusive[:, 1] - own_inclusive[1], 0.0)),
        0.0,
    )
    into_forward = jnp.einsum(
        "nh,nhde->hde", forward_weight, pieces[0], precision=lax.Precision.HIGHEST
    )
    into_backward = jnp.einsum(
        "nh,nhde->hde", backward_weight, pieces[1], precision=lax.Precision.HIGHEST
    )
    forward_part = jnp.einsum(
        "ihd,hde->ihe",
        rotated_query,
        into_forward.astype(jnp.bfloat16),
        preferred_element_type=jnp.float32,
    )
    backward_part = jnp.einsum(
        "ihd,hde->ihe",
        rotated_query,
        into_backward.astype(jnp.bfloat16),
        preferred_element_type=jnp.float32,
    )
    mixed_heads = (
        local_part
        + jnp.exp(forward_cum).T[:, :, None] * forward_part
        + jnp.exp(backward_cum).T[:, :, None] * backward_part
    )
    scaled = mixed_heads * lax.rsqrt(
        jnp.mean(mixed_heads * mixed_heads, axis=-1, keepdims=True) + EPS
    )
    scaled = scaled * head_gain.reshape(head_count, HEAD_DIM)
    return (
        jax.nn.silu(gate_rows.astype(jnp.float32))
        * scaled.reshape(row_count, head_count * HEAD_DIM)
    ).astype(jnp.bfloat16)


def local(
    tokens,
    norm_gain,
    outer_gate,
    inner_gate,
    conv_input,
    query_proj,
    key_proj,
    value_proj,
    out_gate,
    conv_taps,
    log_decay,
    head_gain,
    conv_output,
    retention_output,
):
    whole = lax.all_gather(tokens, "tp", axis=1, tiled=True)
    wide = whole.astype(jnp.float32)
    normed = (
        wide * lax.rsqrt(jnp.mean(wide * wide, axis=-1, keepdims=True) + EPS) * norm_gain
    ).astype(jnp.bfloat16)
    row_count = normed.shape[0]
    offsets = lax.axis_index("sp") * row_count + lax.iota(jnp.int32, row_count)
    gathered = (
        lax.all_gather(outer_gate, "sp", axis=0, tiled=True),
        lax.all_gather(inner_gate, "sp", axis=0, tiled=True),
        lax.all_gather(conv_input, "sp", axis=0, tiled=True),
        lax.all_gather(query_proj, "sp", axis=0, tiled=True),
        lax.all_gather(key_proj, "sp", axis=0, tiled=True),
        lax.all_gather(value_proj, "sp", axis=0, tiled=True),
        lax.all_gather(out_gate, "sp", axis=0, tiled=True),
        lax.all_gather(conv_output, "sp", axis=1, tiled=True),
        lax.all_gather(retention_output, "sp", axis=1, tiled=True),
    )
    projected = [
        jnp.dot(normed, weight, preferred_element_type=jnp.float32).astype(jnp.bfloat16)
        for weight in gathered[:7]
    ]
    conv_out = conv_branch(projected[0], projected[1], projected[2], conv_taps)
    ret_out = retention_branch(
        projected[3], projected[4], projected[5], projected[6], log_decay, head_gain, offsets
    )
    conv_weight = gathered[7]
    ret_weight = gathered[8]
    return lax.psum_scatter(
        (
            jnp.dot(conv_out, conv_weight, preferred_element_type=jnp.float32)
            + jnp.dot(ret_out, ret_weight, preferred_element_type=jnp.float32)
        ).astype(jnp.bfloat16),
        "tp",
        scatter_dimension=0,
        tiled=True,
    )


def flipped(place, d):
    if d == 0:
        return place
    if d == 1:
        return place + 1 - 2 * lax.rem(place, 2)
    if d == 2:
        return place + 2 - 4 * lax.rem(lax.div(place, 2), 2)
    return 3 - place


LOG2E = 1.4426950408889634
CLASS_A, CLASS_B, CLASS_OUT = 0, 1, 2


def mixer_kernel(
    planes, group,
    tok_ref, key_w, query_w, value_w, gate_w, inner_w, conv_w, outer_w,
    cout_ref, rout_ref, rate_in, gain_ref, taps_ref, head_gain_ref, turn_ref, base_ref,
    mine_ref, theirs_ref,
    xin, x, w, wo, rates, cums, wide, ssq_out, ssq_in, cosines, sines, decay,
    ef, eb, kf, kb, rq_buf, v_buf, gate_buf, loc, state_f, state_b, pack_out, pack_in, into,
    acc, iv, parts, feat, share,
    own_sem, near_send, near_recv, rate_send, rate_recv, ssq_sem,
    tok_send, tok_recv, half_send, half_recv, far_send, far_recv,
    wo_send, wo_recv, halo_send, halo_recv, pack_send, pack_recv,
    ft_send, ft_recv, share_send, share_recv,
):
    f32, bf16 = jnp.float32, jnp.bfloat16
    own, core = lax.axis_index("sp"), lax.axis_index("tp")
    place, plane = lax.rem(own, group), lax.div(own, group)
    base = plane * group
    length, half = tok_ref.shape
    width = 2 * half
    quarter = half // 2
    rows_in = key_w.shape[0]
    ch = key_w.shape[1] // group
    heads = ch // HEAD_DIM
    all_rows = group * length
    side_rows = cout_ref.shape[0]
    out_cols = cout_ref.shape[1]
    part_cols = group * out_cols
    col_a, col_b = 4 * ch, 3 * ch
    has_up, has_down = plane < planes - 1, plane > 0
    middle = jnp.logical_and(has_up, has_down)
    top = lax.div(plane, planes // 2)
    mesh_id = pl.DeviceIdType.MESH
    chips = [base + flipped(place, d) for d in range(group)]
    partner = (own, 1 - core)
    weights = (key_w, query_w, value_w, gate_w, inner_w, conv_w, outer_w)

    def local_copy(source, target, i):
        return pltpu.make_async_copy(source, target, own_sem.at[i])

    def remote(source, target, send, recv, device):
        return pltpu.make_async_remote_copy(
            src_ref=source, dst_ref=target, send_sem=send, recv_sem=recv,
            device_id=device, device_id_type=mesh_id,
        )

    own_rows = pl.ds(pl.multiple_of(own * rows_in, 128), rows_in)
    own_cols = pl.ds(pl.multiple_of(own * out_cols, 128), out_cols)
    kept = [local_copy(tok_ref, xin, 0)]
    for j, source in enumerate(weights):
        kept.append(
            local_copy(
                source.at[:, pl.ds(pl.multiple_of(place * ch, 128), ch)],
                w.at[own_rows, pl.ds(j * ch, ch)], 1 + j,
            )
        )
    kept.append(local_copy(cout_ref, wo.at[pl.ds(0, side_rows), own_cols], 8))
    kept.append(local_copy(rout_ref, wo.at[pl.ds(side_rows, side_rows), own_cols], 9))
    kept.append(local_copy(rate_in, rates.at[place], 10))
    for copy in kept:
        copy.start()

    barrier = pltpu.get_barrier_semaphore()

    def greet(target):
        pl.semaphore_signal(barrier, inc=1, device_id=target, device_id_type=mesh_id)

    for d in range(1, group):
        greet((chips[d], core))
    greet(partner)
    for k in range(1, planes):
        greet((lax.rem(own + k * group, planes * group), core))
    pl.semaphore_wait(barrier, group + planes - 1)

    near = {}

    def send_near(j, d):
        to = flipped(place, d)
        near[(j, d)] = remote(
            weights[j].at[:, pl.ds(pl.multiple_of(to * ch, 128), ch)],
            w.at[own_rows, pl.ds(j * ch, ch)],
            near_send.at[j, d], near_recv.at[j, d], (chips[d], core),
        )
        near[(j, d)].start()

    for d in range(1, group):
        for j in range(4):
            send_near(j, d)
    rate_moves = [
        remote(rate_in, rates.at[place], rate_send.at[d], rate_recv.at[d], (chips[d], core))
        for d in range(1, group)
    ]
    for copy in rate_moves:
        copy.start()
    for d in range(1, group):
        for j in range(4, 7):
            send_near(j, d)

    def far(kind, direction, q, d):
        if kind == CLASS_OUT:
            block = wo.at[:, pl.ds(pl.multiple_of((q * group + place) * out_cols, 128), out_cols)]
        else:
            start = pl.multiple_of((q * group + flipped(place, d)) * rows_in, 128)
            cols = pl.ds(0, col_a) if kind == CLASS_A else pl.ds(col_a, col_b)
            block = w.at[pl.ds(start, rows_in), cols]
        target = own + group if direction == 0 else own - group
        return remote(
            block, block, far_send.at[kind, direction, q, d], far_recv.at[kind, q, d], (target, core)
        )

    def places_of(kind):
        return 1 if kind == CLASS_OUT else group

    def own_far(kind, d):
        pl.when(has_up)(lambda: far(kind, 0, plane, d).start())
        pl.when(has_down)(lambda: far(kind, 1, plane, d).start())

    def source_plane(r):
        if r == 0:
            return plane
        if r == 1:
            return plane + 1 - 2 * lax.rem(plane, 2)
        return r + top * (planes - 1 - 2 * r)

    def arrive(kind, r, only=None):
        q = source_plane(r)

        def take():
            for d in range(places_of(kind)):
                far(kind, 0, q, d).wait_recv()
                pl.when(jnp.logical_and(q < plane, has_up))(
                    lambda d=d: far(kind, 0, q, d).start()
                )
                pl.when(jnp.logical_and(q > plane, has_down))(
                    lambda d=d: far(kind, 1, q, d).start()
                )

        if only is None:
            take()
        else:
            pl.when(only)(take)

    ends = jnp.logical_not(middle)

    tile = length // 4
    kept[0].wait()
    for j in range(4):
        kept[1 + j].wait()
    own_far(CLASS_A, 0)

    @pl.loop(0, 4)
    def _(t):
        rows = pl.ds(pl.multiple_of(t * tile, tile), tile)
        value = xin[rows, :].astype(f32)
        value = value * value
        total = value[:, :128]
        for c in range(1, half // 128):
            total = total + value[:, c * 128 : (c + 1) * 128]
        ssq_out[rows, :] = total

    ssq_move = remote(ssq_out, ssq_in, ssq_sem.at[0], ssq_sem.at[1], partner)
    ssq_move.start()
    ssq_move.wait_recv()
    own_half = pl.multiple_of(core * half, 128)

    @pl.loop(0, 4)
    def _(t):
        rows = pl.ds(pl.multiple_of(t * tile, tile), tile)
        total = jnp.sum(ssq_out[rows, :] + ssq_in[rows, :], axis=-1, keepdims=True)
        scale = lax.rsqrt(total / width + EPS)
        value = xin[rows, :].astype(f32) * scale * gain_ref[:, pl.ds(own_half, half)]
        x[pl.ds(pl.multiple_of(place * length + t * tile, tile), tile), pl.ds(own_half, half)] = (
            value.astype(bf16)
        )

    def span_rows(s):
        return pl.ds(pl.multiple_of(s * length, 128), length)

    def piece(d, which):
        return x.at[
            span_rows(flipped(place, d)),
            pl.ds(pl.multiple_of(core * half + which * quarter, 128), quarter),
        ]

    tokens = {}

    def send_piece(which, d_from, hop):
        d_there = d_from + hop
        tokens[(which, d_there)] = remote(
            piece(d_from, which), piece(d_from, which),
            tok_send.at[which, d_there], tok_recv.at[which, d_there], (chips[hop], core),
        )
        tokens[(which, d_there)].start()

    def send_half(d):
        block = x.at[span_rows(flipped(place, d)), pl.ds(own_half, half)]
        remote(block, block, half_send.at[d], half_recv.at[d], partner).start()

    send_piece(0, 0, 1)
    send_piece(1, 0, 2)
    send_piece(1, 0, 1)
    send_piece(0, 0, 2)
    send_half(0)

    for d in range(1, group):
        for j in range(4):
            near[(j, d)].wait_recv()
        own_far(CLASS_A, d)

    kept[10].wait()
    for copy in rate_moves:
        copy.wait_recv()
    for s in range(group):
        for way in range(2):
            for h in range(heads):
                cums[pl.ds(s * 8 + way * heads + h, 1), :] = rates[
                    s, way, pl.ds(heads * place + h, 1), :
                ]
        cums[pl.ds(s * 8 + 2 * heads, 8 - 2 * heads), :] = jnp.zeros(
            (8 - 2 * heads, length), f32
        )
    lanes = lax.broadcasted_iota(jnp.int32, (group * 8, length), 1)
    kinds = lax.rem(lax.broadcasted_iota(jnp.int32, (group * 8, length), 0), 8)
    running = cums[...] * LOG2E
    step = 1
    while step < length:
        ahead = jnp.where(lanes >= step, pltpu.roll(running, step, 1), 0.0)
        behind = jnp.where(lanes < length - step, pltpu.roll(running, length - step, 1), 0.0)
        running = running + jnp.where(kinds < heads, ahead, behind)
        step *= 2
    cums[...] = running
    wide[...] = jnp.zeros_like(wide)
    first_head = lax.broadcasted_iota(jnp.int32, (length, ch), 1) < HEAD_DIM
    lane_in_head = lax.rem(lax.broadcasted_iota(jnp.int32, (length, ch), 1), HEAD_DIM)
    leading = lane_in_head < HEAD_DIM // 2

    @pl.loop(0, group)
    def _(s):
        sums = cums[pl.ds(pl.multiple_of(s * 8, 8), 8), :]
        wide[0:8, :] = sums
        columns = wide[...].T
        cf = [columns[:, h : h + 1] for h in range(heads)]
        rb = [columns[:, heads + h : heads + h + 1] for h in range(heads)]
        cf_wide = jnp.where(first_head, cf[0], cf[1])
        rb_wide = jnp.where(first_head, rb[0], rb[1])
        ef[s] = jnp.exp2(cf_wide)
        eb[s] = jnp.exp2(rb_wide)
        kf[s] = jnp.exp2(cf_wide[length - 1 : length, :] - cf_wide)
        kb[s] = jnp.exp2(rb_wide[0:1, :] - rb_wide)
        row_at = lax.broadcasted_iota(jnp.int32, (length, length), 0)
        col_at = lax.broadcasted_iota(jnp.int32, (length, length), 1)
        for h in range(heads):
            spread = jnp.where(
                col_at <= row_at, cf[h] - sums[h : h + 1, :], rb[h] - sums[heads + h : heads + h + 1, :]
            )
            decay[s, h] = jnp.exp2(spread)
        turn = base_ref[base + s]
        cos_0, sin_0 = turn[0:1, :], turn[1:2, :]
        cos_i, sin_i = turn_ref[0], turn_ref[1]
        cosines[s] = cos_0 * cos_i - sin_0 * sin_i
        angle_sine = sin_0 * cos_i + cos_0 * sin_i
        sines[s] = jnp.where(leading, -angle_sine, angle_sine)

    arrive(CLASS_A, 1)
    for d in range(1, group):
        for j in range(4, 7):
            near[(j, d)].wait_recv()
    for j in range(4, 7):
        kept[1 + j].wait()
    for d in range(group):
        own_far(CLASS_B, d)
    tokens[(0, 1)].wait_recv()
    send_piece(0, 1, 2)
    tokens[(1, 2)].wait_recv()
    send_piece(1, 2, 1)
    arrive(CLASS_A, 2)
    tokens[(1, 1)].wait_recv()
    send_half(1)
    tokens[(0, 2)].wait_recv()
    send_half(2)
    arrive(CLASS_A, 3)
    arrive(CLASS_B, 1, middle)
    arrive(CLASS_B, 2, middle)
    kept[8].wait()
    kept[9].wait()
    pl.when(ends)(lambda: own_far(CLASS_OUT, 0))

    def out_piece(r, d, which):
        start = pl.multiple_of((source_plane(r) * group + flipped(place, d)) * out_cols, 128)
        return wo.at[pl.ds(which * side_rows, side_rows), pl.ds(start, out_cols)]

    def out_move(r, which, d_there, hop):
        block = out_piece(r, d_there - hop, which)
        return remote(
            block, block, wo_send.at[r, which, d_there], wo_recv.at[r, which, d_there],
            (chips[hop], core),
        )

    def out_landed(r, which, d):
        block = out_piece(r, d, which)
        remote(
            block, block, wo_send.at[r, which, d], wo_recv.at[r, which, d], (chips[1], core)
        ).wait_recv()

    def spread_out(r):
        for which, hop in ((0, 1), (1, 2), (1, 1), (0, 2)):
            out_move(r, which, hop, hop).start()

    def relay_out(r):
        out_landed(r, 0, 1)
        out_move(r, 0, 3, 2).start()
        out_landed(r, 1, 2)
        out_move(r, 1, 3, 1).start()

    def finish_out(r):
        for which, d in ((1, 1), (0, 2), (0, 3), (1, 3)):
            out_landed(r, which, d)

    def wait_half(d):
        block = x.at[
            span_rows(flipped(place, d)), pl.ds(pl.multiple_of((1 - core) * half, 128), half)
        ]
        remote(block, block, half_send.at[d], half_recv.at[d], partner).wait_recv()

    spread_out(0)
    wait_half(0)

    def one_span(s):
        rows = span_rows(s)
        held = jnp.dot(x[rows, :], w[:, 0:col_a], preferred_element_type=f32)
        cosine, sine = cosines[s], sines[s]

        def turned(value):
            value = value.astype(bf16).astype(f32)
            other = jnp.where(
                leading,
                pltpu.roll(value, ch - HEAD_DIM // 2, 1),
                pltpu.roll(value, HEAD_DIM // 2, 1),
            )
            return value * cosine + other * sine

        rk = (turned(held[:, 0:ch]) * HEAD_DIM ** (-0.5)).astype(bf16).astype(f32)
        rq = turned(held[:, ch : 2 * ch]).astype(bf16)
        value = held[:, 2 * ch : 3 * ch].astype(bf16)
        rq_buf[s] = rq
        v_buf[s] = value
        gate_buf[s] = held[:, 3 * ch : 4 * ch].astype(bf16)
        value_wide = value.astype(f32)
        found = None
        for h in range(heads):
            in_head = first_head if h == 0 else jnp.logical_not(first_head)
            key_head = jnp.where(in_head, rk, 0.0).astype(bf16)
            value_head = jnp.where(in_head, value_wide, 0.0).astype(bf16)
            scores = lax.dot_general(
                rq, key_head, (((1,), (1,)), ((), ())), preferred_element_type=f32
            )
            probs = (scores * decay[s, h]).astype(bf16)
            part = jnp.dot(probs, value_head, preferred_element_type=f32)
            found = part if found is None else found + part
        loc[s] = found
        same_head = (
            lax.div(lax.broadcasted_iota(jnp.int32, (ch, ch), 0), HEAD_DIM)
            == lax.div(lax.broadcasted_iota(jnp.int32, (ch, ch), 1), HEAD_DIM)
        )
        for table, target in ((kf, state_f), (kb, state_b)):
            keys = (rk * table[s]).astype(bf16)
            state = lax.dot_general(
                keys, value, (((0,), (0,)), ((), ())), preferred_element_type=f32
            )
            target[s] = jnp.where(same_head, state, 0.0)

    halo_rows = 16
    halos = [
        remote(
            x.at[pl.ds(all_rows - halo_rows, halo_rows), :], x.at[pl.ds(all_rows, halo_rows), :],
            halo_send.at[0], halo_recv.at[0], (own + group, core),
        ),
        remote(
            x.at[pl.ds(0, halo_rows), :], x.at[pl.ds(all_rows + halo_rows, halo_rows), :],
            halo_send.at[1], halo_recv.at[1], (own - group, core),
        ),
    ]
    blank = jnp.zeros((halo_rows, width), bf16)

    @pl.when(jnp.logical_not(has_down))
    def _():
        x[pl.ds(all_rows, halo_rows), :] = blank

    @pl.when(jnp.logical_not(has_up))
    def _():
        x[pl.ds(all_rows + halo_rows, halo_rows), :] = blank

    @pl.loop(0, group)
    def _(d):
        @pl.when(d == 1)
        def _():
            tokens[(0, 3)].wait_recv()
            tokens[(1, 3)].wait_recv()
            send_half(3)
            wait_half(1)

        @pl.when(d == 2)
        def _():
            wait_half(2)
            relay_out(0)

        @pl.when(d == 3)
        def _():
            wait_half(3)
            pl.when(has_up)(lambda: halos[0].start())
            pl.when(has_down)(lambda: halos[1].start())
            arrive(CLASS_B, 3, middle)

        one_span(lax.rem(lax.rem(place, 2) + lax.rem(d, 2), 2)
                 + 2 * lax.rem(lax.div(place, 2) + lax.div(d, 2), 2))

    def scan_states(state, table, at, order, target):
        passed, inside, reach = jnp.zeros((ch, ch), f32), {}, {}
        over = jnp.ones((1, ch), f32)
        for s in order:
            inside[s], reach[s] = passed, over
            factor = table[s, at : at + 1, :]
            passed = factor * passed + state[s]
            over = over * factor
        pack_out[target, 0:ch, :] = passed
        pack_out[target, ch : ch + 8, :] = jnp.broadcast_to(over, (8, ch))
        return inside, reach

    ahead_in, ahead_reach = scan_states(state_f, ef, length - 1, range(group), 0)
    back_in, back_reach = scan_states(state_b, eb, 0, range(group)[::-1], 1)

    def pack_move(way, k):
        to = own + k * group if way == 0 else own - k * group
        return remote(
            pack_out.at[way], pack_in.at[way, k - 1],
            pack_send.at[way, k], pack_recv.at[way, k], (to, core),
        )

    def gives(way, k):
        return plane + k < planes if way == 0 else plane - k >= 0

    def takes(way, k):
        return gives(1 - way, k)

    for k in range(1, planes):
        for way in range(2):
            pl.when(gives(way, k))(lambda way=way, k=k: pack_move(way, k).start())
    pl.when(middle)(lambda: own_far(CLASS_OUT, 0))

    arrive(CLASS_B, 1, ends)
    arrive(CLASS_B, 2, ends)
    pl.when(has_down)(lambda: halos[0].wait_recv())
    pl.when(has_up)(lambda: halos[1].wait_recv())
    depth = group * rows_in
    most = (planes - 1) * depth
    early = pl.multiple_of(top * depth, 128)
    late = pl.multiple_of((1 - top) * most, 128)
    blocks = 5
    block = (all_rows + 2 * halo_rows) // blocks

    @pl.loop(0, blocks)
    def _(t):
        rows = pl.ds(pl.multiple_of(t * block, 16), block)
        acc[rows, :] = jnp.dot(
            x[rows, pl.ds(early, most)], w[pl.ds(early, most), col_a : col_a + col_b],
            preferred_element_type=f32,
        )

    arrive(CLASS_B, 3, ends)

    @pl.loop(0, blocks)
    def _(t):
        rows = pl.ds(pl.multiple_of(t * block, 16), block)
        held = acc[rows, :] + jnp.dot(
            x[rows, pl.ds(late, depth)], w[pl.ds(late, depth), col_a : col_a + col_b],
            preferred_element_type=f32,
        )
        held = held.astype(bf16).astype(f32)
        iv[pl.ds(pl.multiple_of(t * block + 8, 8), block), :] = (
            (held[:, 0:ch] * held[:, ch : 2 * ch]).astype(bf16).astype(f32)
        )
        acc[rows, 2 * ch : 3 * ch] = held[:, 2 * ch : 3 * ch]

    iv[7:8, :] = iv[all_rows + halo_rows + 7 : all_rows + halo_rows + 8, :]
    iv[all_rows + 8 : all_rows + 9, :] = iv[all_rows + halo_rows + 8 : all_rows + halo_rows + 9, :]
    own_taps = taps_ref[:, pl.ds(pl.multiple_of(place * ch, 128), ch)]
    for s in range(group):
        at = s * length
        near_sum = (
            own_taps[0:1, :] * iv[at + 7 : at + 7 + length, :]
            + own_taps[1:2, :] * iv[at + 8 : at + 8 + length, :]
            + own_taps[2:3, :] * iv[at + 9 : at + 9 + length, :]
        )
        parts[0, s] = (acc[at : at + length, 2 * ch : 3 * ch] * near_sum).astype(bf16)

    def feature_cols(kind):
        return pl.ds(pl.multiple_of(kind * side_rows + place * ch, 128), ch)

    def feature_move(kind, d, s, to):
        return remote(
            parts.at[kind, s], feat.at[:, feature_cols(kind)],
            ft_send.at[kind, d], ft_recv.at[kind, d], (to, core),
        )

    for d in (3, 1, 2):
        feature_move(0, d, flipped(place, d), chips[d]).start()
    feat[:, feature_cols(0)] = parts[0, place]

    arrive(CLASS_OUT, 1)
    spread_out(1)

    incoming = []
    for way in range(2):
        into[way] = jnp.zeros((ch, ch), f32)
        into[way + 2] = jnp.ones((ch, ch), f32)
        for k in range(1, planes):
            @pl.when(takes(way, k))
            def _(way=way, k=k):
                pack_move(way, k).wait_recv()
                into[way] = into[way] + into[way + 2] * pack_in[way, k - 1, 0:ch, :]
                into[way + 2] = into[way + 2] * pack_in[way, k - 1, ch : ch + 1, :]
        incoming.append(into[way])
    for s in range(group):
        state_f[s] = ahead_in[s] + ahead_reach[s] * incoming[0]
        state_b[s] = back_in[s] + back_reach[s] * incoming[1]

    @pl.loop(0, group)
    def _(i):
        d = group - 1 - i
        s = (lax.rem(lax.rem(place, 2) + lax.rem(d, 2), 2)
             + 2 * lax.rem(lax.div(place, 2) + lax.div(d, 2), 2))
        query = rq_buf[s]
        mix = (
            loc[s]
            + ef[s] * jnp.dot(query, state_f[s].astype(bf16), preferred_element_type=f32)
            + eb[s] * jnp.dot(query, state_b[s].astype(bf16), preferred_element_type=f32)
        )
        squares = mix * mix
        first = jnp.sum(jnp.where(first_head, squares, 0.0), axis=-1, keepdims=True)
        second = jnp.sum(jnp.where(first_head, 0.0, squares), axis=-1, keepdims=True)
        scale = lax.rsqrt(jnp.where(first_head, first, second) / HEAD_DIM + EPS)
        gate = gate_buf[s].astype(f32)
        gain = head_gain_ref[:, pl.ds(pl.multiple_of(place * ch, 128), ch)]
        parts[1, s] = (gate / (1.0 + jnp.exp(-gate)) * (mix * scale * gain)).astype(bf16)

        @pl.when(d > 0)
        def _():
            feature_move(1, d, s, base + s).start()

    feat[:, feature_cols(1)] = parts[1, place]

    relay_out(1)
    arrive(CLASS_OUT, 2)
    spread_out(2)
    relay_out(2)
    arrive(CLASS_OUT, 3)
    spread_out(3)
    for kind in range(2):
        for d in (1, 2, 3):
            feature_move(kind, d, flipped(place, d), chips[d]).wait_recv()

    my_rows = length // 2
    shares = []

    def project(r):
        cols = pl.ds(pl.multiple_of(source_plane(r) * part_cols, 128), part_cols)

        def rows_of(c):
            return jnp.dot(
                feat[pl.ds(pl.multiple_of(c * my_rows, 128), my_rows), :], wo[:, cols],
                preferred_element_type=f32,
            ).astype(bf16)

        share[:, cols] = rows_of(1 - core)
        move = remote(
            share.at[:, cols], theirs_ref.at[:, cols], share_send.at[r], share_recv.at[r], partner
        )
        move.start()
        shares.append(move)
        mine_ref[:, cols] = rows_of(core)

    finish_out(0)
    project(0)
    finish_out(1)
    project(1)
    relay_out(3)
    finish_out(2)
    project(2)
    finish_out(3)
    project(3)

    for move in shares:
        move.wait()
    for copy in near.values():
        copy.wait_send()
    for copy in rate_moves:
        copy.wait_send()
    ssq_move.wait_send()
    for copy in tokens.values():
        copy.wait_send()
    for d in range(group):
        halves_block = x.at[span_rows(flipped(place, d)), pl.ds(own_half, half)]
        remote(halves_block, halves_block, half_send.at[d], half_recv.at[d], partner).wait_send()
    for r in range(planes):
        for which, d, hop in ((0, 1, 1), (1, 1, 1), (0, 2, 2), (1, 2, 2), (0, 3, 2), (1, 3, 1)):
            out_move(r, which, d, hop).wait_send()
    pl.when(has_up)(lambda: halos[0].wait_send())
    pl.when(has_down)(lambda: halos[1].wait_send())
    for k in range(1, planes):
        for way in range(2):
            pl.when(gives(way, k))(lambda way=way, k=k: pack_move(way, k).wait_send())
    for kind in range(2):
        for d in range(1, group):
            feature_move(kind, d, flipped(place, d), chips[d]).wait_send()
    for kind in range(3):
        for q in range(planes):
            for d in range(places_of(kind)):
                pl.when(jnp.logical_and(q <= plane, has_up))(
                    lambda kind=kind, q=q, d=d: far(kind, 0, q, d).wait_send()
                )
                pl.when(jnp.logical_and(q >= plane, has_down))(
                    lambda kind=kind, q=q, d=d: far(kind, 1, q, d).wait_send()
                )


def turn_tables(spans, length, channels):
    half_dim = HEAD_DIM // 2
    frequency = THETA ** (-2.0 * (np.arange(channels) % half_dim) / HEAD_DIM)
    inner = np.arange(length)[:, None] * frequency
    outer = (np.arange(spans) * length)[:, None] * frequency
    turn = np.stack([np.cos(inner), np.sin(inner)])
    start = np.zeros((spans, 8, channels))
    start[:, 0], start[:, 1] = np.cos(outer), np.sin(outer)
    return turn.astype(np.float32), start.astype(np.float32)


def mixer(planes, group, arrays):
    (
        tokens, norm_gain, outer_gate, inner_gate, conv_input, query_proj, key_proj, value_proj,
        out_gate, conv_taps, log_decay, head_gain, conv_output, retention_output,
    ) = arrays
    f32, bf16 = jnp.float32, jnp.bfloat16
    length, half = tokens.shape
    width = 2 * half
    ch = outer_gate.shape[1] // group
    heads = ch // HEAD_DIM
    rows, side = group * length, conv_output.shape[0]
    turn, start = turn_tables(planes * group, length, ch)
    dma = pltpu.SemaphoreType.DMA
    vmem, anywhere = pl.BlockSpec(memory_space=pltpu.VMEM), pl.BlockSpec(memory_space=pl.ANY)
    v = pltpu.VMEM
    result = jax.ShapeDtypeStruct((length // 2, width), bf16)
    table = v((group, length, ch), f32)
    mine, theirs = pl.pallas_call(
        functools.partial(mixer_kernel, planes, group),
        out_shape=(result, result),
        in_specs=[anywhere] * 11 + [vmem] * 5,
        out_specs=[vmem, vmem],
        scratch_shapes=[
            v((length, half), bf16), v((rows + 32, width), bf16), v((width, 7 * ch), bf16),
            v((2 * side, width), bf16), v((group,) + log_decay.shape, f32),
            v((8 * group, length), f32), v((128, length), f32),
            v((length, 128), f32), v((length, 128), f32),
            table, table, v((group, heads, length, length), f32),
            table, table, table, table,
            v((group, length, ch), bf16), v((group, length, ch), bf16), v((group, length, ch), bf16),
            table, v((group, ch, ch), f32), v((group, ch, ch), f32),
            v((2, ch + 8, ch), f32), v((2, planes - 1, ch + 8, ch), f32), v((4, ch, ch), f32),
            v((rows + 32, 3 * ch), f32), v((rows + 48, ch), f32),
            v((2, group, length, ch), bf16), v((length, 2 * side), bf16),
            v((length // 2, width), bf16),
            dma((11,)), dma((7, group)), dma((7, group)), dma((group,)), dma((group,)), dma((2,)),
            dma((2, group)), dma((2, group)), dma((group,)), dma((group,)),
            dma((3, 2, planes, group)), dma((3, planes, group)),
            dma((planes, 2, group)), dma((planes, 2, group)), dma((2,)), dma((2,)),
            dma((2, planes)), dma((2, planes)), dma((2, group)), dma((2, group)),
            dma((planes,)), dma((planes,)),
        ],
        compiler_params=pltpu.CompilerParams(
            collective_id=0, has_side_effects=True, vmem_limit_bytes=60 * 2**20
        ),
    )(
        tokens, key_proj, query_proj, value_proj, out_gate, inner_gate, conv_input, outer_gate,
        conv_output, retention_output, log_decay, norm_gain.reshape(1, -1), conv_taps,
        head_gain.reshape(1, -1), jnp.asarray(turn), jnp.asarray(start),
    )
    return (mine.astype(f32) + theirs.astype(f32)).astype(bf16)


LANES = 128

def plan(*arrays):
    spans, cores = lax.axis_size("sp"), lax.axis_size("tp")
    group = arrays[2].shape[1] // LANES
    planes = spans // group
    fits = (
        cores == 2
        and group == 4
        and planes * group == spans
        and planes == 2 * cores
        and arrays[0].shape[1] == 2 * group * arrays[2].shape[0]
    )
    return mixer(planes, group, arrays) if fits else local(*arrays)


def solution(mesh):
    return jax.shard_map(
        plan,
        mesh=mesh,
        in_specs=(
            P("sp", "tp"),
            P(),
            P("sp", "tp"),
            P("sp", "tp"),
            P("sp", "tp"),
            P("sp", "tp"),
            P("sp", "tp"),
            P("sp", "tp"),
            P("sp", "tp"),
            P(None, "tp"),
            P(None, "tp", "sp"),
            P("tp"),
            P("tp", "sp"),
            P("tp", "sp"),
        ),
        out_specs=P(("sp", "tp"), None),
        check_vma=False,
    )
```

profile of v0, /device:TPU:0, one launch (start us, length us, event | category | flops | bytes accessed | tf_op | source)
XLA Modules:
  0.0 125.4 jit_solution(13767503391135626720)
XLA Ops:
  0.0 122.5 %shard_map.154 = (bf16[256,2048]{1,0:T(8,128)(2,1)}, bf16[256,2048]{1,0:T(8,128)(2,1)}) custom-call(bf16[512,1024]{1,0:T(8,128)(2,1)} %tok_ref.1, bf16[128,512]{1,0:T(8,128)(2,1)} %key_w.1, bf16[128,512]{1,0:T(8,128)(2,1)} %query_w.1, bf16[128,512]{1,0:T(8,128)(2,1)} %value_w.1, bf16[128,512]{1,0:T(8,128)(2,1)} %gate_w.1, bf16[128,512]{1,0:T(8,128)(2,1)} %inner_w.1, ...), custom_call_target="tpu_custom_call" | custom-call | tf_op jit(solution)/shard_map/pallas_call | solution.py:880
  122.5 2.9 %add_convert_fusion = bf16[256,2048]{1,0:T(8,128)(2,1)} fusion(bf16[256,2048]{1,0:T(8,128)(2,1)} %get-tuple-element.8, bf16[256,2048]{1,0:T(8,128)(2,1)} %get-tuple-element.7), kind=kLoop, calls=%fused_computation | loop fusion | flops 2097152 | bytes 3145728 | tf_op jit(solution)/shard_map/convert_element_type | solution.py:913
where the time goes:
time: 126 us; the launch traced here: 125 us
  Pallas kernels  122 us (97%)
  other arithmetic  2.91 us (2%)
    pallas_call x1, Pallas kernels, mixer(): pl.pallas_call(functools.partial(mixer_kernel, planes, group), out_shape=...  122 us
    convert_element_type x1, other arithmetic, mixer(): return (mine.astype(f32) + theirs.astype(f32)).astype(bf16)  2.91 us

commit v1 on v0

--- a/solution.py
+++ b/solution.py
@@ -228,13 +228,13 @@
 def mixer_kernel(
     planes, group,
     tok_ref, key_w, query_w, value_w, gate_w, inner_w, conv_w, outer_w,
-    cout_ref, rout_ref, rate_in, gain_ref, taps_ref, head_gain_ref, turn_ref, base_ref,
-    mine_ref, theirs_ref,
-    xin, x, w, wo, rates, cums, wide, ssq_out, ssq_in, cosines, sines, decay,
+    cout_ref, rout_ref, rate_in, gain_in, taps_in, head_gain_in, turn_in, base_in,
+    out_ref, gain_ref, taps_ref, head_gain_ref, turn_ref, base_ref,
+    xin, x, w, wo, rate_own, rate_pack, rates, cums, wide, ssq_out, ssq_in, cosines, sines, decay,
     ef, eb, kf, kb, rq_buf, v_buf, gate_buf, loc, state_f, state_b, pack_out, pack_in, into,
-    acc, iv, parts, feat, share,
+    acc, iv, parts, feat, share, theirs,
     own_sem, near_send, near_recv, rate_send, rate_recv, ssq_sem,
-    tok_send, tok_recv, half_send, half_recv, far_send, far_recv,
+    tok_send, tok_recv, half_send, half_recv, far_send, far_recv, out_recv,
     wo_send, wo_recv, halo_send, halo_recv, pack_send, pack_recv,
     ft_send, ft_recv, share_send, share_recv,
 ):
@@ -272,19 +272,33 @@
 
     own_rows = pl.ds(pl.multiple_of(own * rows_in, 128), rows_in)
     own_cols = pl.ds(pl.multiple_of(own * out_cols, 128), out_cols)
-    kept = [local_copy(tok_ref, xin, 0)]
+    kept = [local_copy(tok_ref, xin, 0), local_copy(rate_in, rate_own, 1)]
     for j, source in enumerate(weights):
         kept.append(
             local_copy(
                 source.at[:, pl.ds(pl.multiple_of(place * ch, 128), ch)],
-                w.at[own_rows, pl.ds(j * ch, ch)], 1 + j,
+                w.at[own_rows, pl.ds(j * ch, ch)], 2 + j // 4,
             )
         )
-    kept.append(local_copy(cout_ref, wo.at[pl.ds(0, side_rows), own_cols], 8))
-    kept.append(local_copy(rout_ref, wo.at[pl.ds(side_rows, side_rows), own_cols], 9))
-    kept.append(local_copy(rate_in, rates.at[place], 10))
-    for copy in kept:
+    kept.append(local_copy(cout_ref, wo.at[pl.ds(0, side_rows), own_cols], 4))
+    kept.append(local_copy(rout_ref, wo.at[pl.ds(side_rows, side_rows), own_cols], 4))
+    place_cols = pl.ds(pl.multiple_of(place * ch, 128), ch)
+    small = [
+        local_copy(gain_in, gain_ref, 5),
+        local_copy(taps_in, taps_ref, 6),
+        local_copy(head_gain_in, head_gain_ref, 7),
+        local_copy(turn_in, turn_ref, 8),
+        local_copy(base_in.at[pl.ds(base, group)], base_ref, 9),
+    ]
+    for copy in kept + small:
         copy.start()
+
+    def class_cols(kind):
+        return pl.ds(0, col_a) if kind == CLASS_A else pl.ds(col_a, col_b)
+
+    def own_here(kind):
+        block = wo.at[:, own_cols] if kind == CLASS_OUT else w.at[own_rows, class_cols(kind)]
+        local_copy(block, block, 2 + kind).wait()
 
     barrier = pltpu.get_barrier_semaphore()
 
@@ -298,24 +312,43 @@
         greet((lax.rem(own + k * group, planes * group), core))
     pl.semaphore_wait(barrier, group + planes - 1)
 
-    near = {}
-
     def send_near(j, d):
         to = flipped(place, d)
-        near[(j, d)] = remote(
+        remote(
             weights[j].at[:, pl.ds(pl.multiple_of(to * ch, 128), ch)],
             w.at[own_rows, pl.ds(j * ch, ch)],
-            near_send.at[j, d], near_recv.at[j, d], (chips[d], core),
-        )
-        near[(j, d)].start()
+            near_send.at[j // 4, d - 1], near_recv.at[j // 4, d - 1], (chips[d], core),
+        ).start()
+
+    def near_block(kind, d):
+        start = pl.multiple_of((base + flipped(place, d)) * rows_in, 128)
+        block = w.at[pl.ds(start, rows_in), class_cols(kind)]
+        return remote(
+            block, block, near_send.at[kind, d - 1], near_recv.at[kind, d - 1], (chips[d], core)
+        )
 
     for d in range(1, group):
         for j in range(4):
             send_near(j, d)
-    rate_moves = [
-        remote(rate_in, rates.at[place], rate_send.at[d], rate_recv.at[d], (chips[d], core))
-        for d in range(1, group)
-    ]
+
+    rate_rows = 2 * heads
+    kept[1].wait()
+    rate_moves = []
+    for d in range(group):
+        to = flipped(place, d)
+        for way in range(2):
+            for h in range(heads):
+                rate_pack[d, pl.ds(way * heads + h, 1), :] = rate_own[
+                    way, pl.ds(heads * to + h, 1), :
+                ]
+        rate_pack[d, pl.ds(rate_rows, 8 - rate_rows), :] = jnp.zeros((8 - rate_rows, length), f32)
+    for d in range(1, group):
+        rate_moves.append(
+            remote(
+                rate_pack.at[d], rates.at[place], rate_send.at[0], rate_recv.at[d - 1],
+                (chips[d], core),
+            )
+        )
     for copy in rate_moves:
         copy.start()
     for d in range(1, group):
@@ -327,12 +360,22 @@
             block = wo.at[:, pl.ds(pl.multiple_of((q * group + place) * out_cols, 128), out_cols)]
         else:
             start = pl.multiple_of((q * group + flipped(place, d)) * rows_in, 128)
-            cols = pl.ds(0, col_a) if kind == CLASS_A else pl.ds(col_a, col_b)
-            block = w.at[pl.ds(start, rows_in), cols]
+            block = w.at[pl.ds(start, rows_in), class_cols(kind)]
+        landed = out_recv.at[q] if kind == CLASS_OUT else far_recv.at[kind, q, d]
         target = own + group if direction == 0 else own - group
-        return remote(
-            block, block, far_send.at[kind, direction, q, d], far_recv.at[kind, q, d], (target, core)
-        )
+        return remote(block, block, far_send.at[kind, direction, q], landed, (target, core))
+
+    def far_sent(kind, direction, q):
+        if kind == CLASS_OUT:
+            far(kind, direction, q, 0).wait_send()
+        else:
+            block = w.at[
+                pl.ds(pl.multiple_of(q * group * rows_in, 128), group * rows_in), class_cols(kind)
+            ]
+            remote(
+                block, block, far_send.at[kind, direction, q], far_recv.at[kind, q, 0],
+                (own + group, core),
+            ).wait_send()
 
     def places_of(kind):
         return 1 if kind == CLASS_OUT else group
@@ -348,11 +391,11 @@
             return plane + 1 - 2 * lax.rem(plane, 2)
         return r + top * (planes - 1 - 2 * r)
 
-    def arrive(kind, r, only=None):
+    def arrive(kind, r, only=None, blocks=None):
         q = source_plane(r)
 
         def take():
-            for d in range(places_of(kind)):
+            for d in range(places_of(kind)) if blocks is None else blocks:
                 far(kind, 0, q, d).wait_recv()
                 pl.when(jnp.logical_and(q < plane, has_up))(
                     lambda d=d: far(kind, 0, q, d).start()
@@ -370,9 +413,10 @@
 
     tile = length // 4
     kept[0].wait()
-    for j in range(4):
-        kept[1 + j].wait()
+    own_here(CLASS_A)
     own_far(CLASS_A, 0)
+    own_here(CLASS_OUT)
+    own_far(CLASS_OUT, 0)
 
     @pl.loop(0, 4)
     def _(t):
@@ -387,6 +431,7 @@
     ssq_move = remote(ssq_out, ssq_in, ssq_sem.at[0], ssq_sem.at[1], partner)
     ssq_move.start()
     ssq_move.wait_recv()
+    small[0].wait()
     own_half = pl.multiple_of(core * half, 128)
 
     @pl.loop(0, 4)
@@ -414,13 +459,13 @@
         d_there = d_from + hop
         tokens[(which, d_there)] = remote(
             piece(d_from, which), piece(d_from, which),
-            tok_send.at[which, d_there], tok_recv.at[which, d_there], (chips[hop], core),
+            tok_send.at[0], tok_recv.at[which, d_there - 1], (chips[hop], core),
         )
         tokens[(which, d_there)].start()
 
     def send_half(d):
         block = x.at[span_rows(flipped(place, d)), pl.ds(own_half, half)]
-        remote(block, block, half_send.at[d], half_recv.at[d], partner).start()
+        remote(block, block, half_send.at[0], half_recv.at[d], partner).start()
 
     send_piece(0, 0, 1)
     send_piece(1, 0, 2)
@@ -429,22 +474,16 @@
     send_half(0)
 
     for d in range(1, group):
-        for j in range(4):
-            near[(j, d)].wait_recv()
+        near_block(CLASS_A, d).wait_recv()
         own_far(CLASS_A, d)
 
-    kept[10].wait()
+    for copy in small[1:]:
+        copy.wait()
     for copy in rate_moves:
         copy.wait_recv()
+    rates[place] = rate_pack[0]
     for s in range(group):
-        for way in range(2):
-            for h in range(heads):
-                cums[pl.ds(s * 8 + way * heads + h, 1), :] = rates[
-                    s, way, pl.ds(heads * place + h, 1), :
-                ]
-        cums[pl.ds(s * 8 + 2 * heads, 8 - 2 * heads), :] = jnp.zeros(
-            (8 - 2 * heads, length), f32
-        )
+        cums[s * 8 : s * 8 + 8, :] = rates[s]
     lanes = lax.broadcasted_iota(jnp.int32, (group * 8, length), 1)
     kinds = lax.rem(lax.broadcasted_iota(jnp.int32, (group * 8, length), 0), 8)
     running = cums[...] * LOG2E
@@ -480,37 +519,13 @@
                 col_at <= row_at, cf[h] - sums[h : h + 1, :], rb[h] - sums[heads + h : heads + h + 1, :]
             )
             decay[s, h] = jnp.exp2(spread)
-        turn = base_ref[base + s]
+        turn = base_ref[s]
         cos_0, sin_0 = turn[0:1, :], turn[1:2, :]
         cos_i, sin_i = turn_ref[0], turn_ref[1]
         cosines[s] = cos_0 * cos_i - sin_0 * sin_i
         angle_sine = sin_0 * cos_i + cos_0 * sin_i
         sines[s] = jnp.where(leading, -angle_sine, angle_sine)
 
-    arrive(CLASS_A, 1)
-    for d in range(1, group):
-        for j in range(4, 7):
-            near[(j, d)].wait_recv()
-    for j in range(4, 7):
-        kept[1 + j].wait()
-    for d in range(group):
-        own_far(CLASS_B, d)
-    tokens[(0, 1)].wait_recv()
-    send_piece(0, 1, 2)
-    tokens[(1, 2)].wait_recv()
-    send_piece(1, 2, 1)
-    arrive(CLASS_A, 2)
-    tokens[(1, 1)].wait_recv()
-    send_half(1)
-    tokens[(0, 2)].wait_recv()
-    send_half(2)
-    arrive(CLASS_A, 3)
-    arrive(CLASS_B, 1, middle)
-    arrive(CLASS_B, 2, middle)
-    kept[8].wait()
-    kept[9].wait()
-    pl.when(ends)(lambda: own_far(CLASS_OUT, 0))
-
     def out_piece(r, d, which):
         start = pl.multiple_of((source_plane(r) * group + flipped(place, d)) * out_cols, 128)
         return wo.at[pl.ds(which * side_rows, side_rows), pl.ds(start, out_cols)]
@@ -518,14 +533,14 @@
     def out_move(r, which, d_there, hop):
         block = out_piece(r, d_there - hop, which)
         return remote(
-            block, block, wo_send.at[r, which, d_there], wo_recv.at[r, which, d_there],
+            block, block, wo_send.at[0], wo_recv.at[r, which, d_there - 1],
             (chips[hop], core),
         )
 
     def out_landed(r, which, d):
         block = out_piece(r, d, which)
         remote(
-            block, block, wo_send.at[r, which, d], wo_recv.at[r, which, d], (chips[1], core)
+            block, block, wo_send.at[0], wo_recv.at[r, which, d - 1], (chips[1], core)
         ).wait_recv()
 
     def spread_out(r):
@@ -546,10 +561,50 @@
         block = x.at[
             span_rows(flipped(place, d)), pl.ds(pl.multiple_of((1 - core) * half, 128), half)
         ]
-        remote(block, block, half_send.at[d], half_recv.at[d], partner).wait_recv()
-
+        remote(block, block, half_send.at[0], half_recv.at[d], partner).wait_recv()
+
+    for d in range(group):
+        arrive(CLASS_A, 1, middle, (d,))
+        arrive(CLASS_A, 2, middle, (d,))
+    arrive(CLASS_OUT, 1, middle)
+    for d in range(1, group):
+        near_block(CLASS_B, d).wait_recv()
+    own_here(CLASS_B)
+
+    @pl.when(ends)
+    def _():
+        for d in range(group):
+            own_far(CLASS_B, d)
+
+    tokens[(0, 1)].wait_recv()
+    send_piece(0, 1, 2)
+    tokens[(1, 2)].wait_recv()
+    send_piece(1, 2, 1)
     spread_out(0)
+    arrive(CLASS_OUT, 1, ends)
+    spread_out(1)
+    arrive(CLASS_A, 3, middle)
+    arrive(CLASS_OUT, 2, middle)
+
+    @pl.when(middle)
+    def _():
+        for d in range(group):
+            own_far(CLASS_B, d)
+
+    tokens[(1, 1)].wait_recv()
+    send_half(1)
+    tokens[(0, 2)].wait_recv()
+    send_half(2)
+    for r in range(1, planes):
+        arrive(CLASS_A, r, ends)
+    arrive(CLASS_OUT, 3, middle)
+    arrive(CLASS_B, 1, middle)
     wait_half(0)
+
+    same_head = (
+        lax.div(lax.broadcasted_iota(jnp.int32, (ch, ch), 0), HEAD_DIM)
+        == lax.div(lax.broadcasted_iota(jnp.int32, (ch, ch), 1), HEAD_DIM)
+    )
 
     def one_span(s):
         rows = span_rows(s)
@@ -584,10 +639,6 @@
             part = jnp.dot(probs, value_head, preferred_element_type=f32)
             found = part if found is None else found + part
         loc[s] = found
-        same_head = (
-            lax.div(lax.broadcasted_iota(jnp.int32, (ch, ch), 0), HEAD_DIM)
-            == lax.div(lax.broadcasted_iota(jnp.int32, (ch, ch), 1), HEAD_DIM)
-        )
         for table, target in ((kf, state_f), (kb, state_b)):
             keys = (rk * table[s]).astype(bf16)
             state = lax.dot_general(
@@ -628,14 +679,15 @@
         @pl.when(d == 2)
         def _():
             wait_half(2)
-            relay_out(0)
 
         @pl.when(d == 3)
         def _():
             wait_half(3)
             pl.when(has_up)(lambda: halos[0].start())
             pl.when(has_down)(lambda: halos[1].start())
-            arrive(CLASS_B, 3, middle)
+            relay_out(0)
+            arrive(CLASS_OUT, 2, ends)
+            spread_out(2)
 
         one_span(lax.rem(lax.rem(place, 2) + lax.rem(d, 2), 2)
                  + 2 * lax.rem(lax.div(place, 2) + lax.div(d, 2), 2))
@@ -648,8 +700,11 @@
             factor = table[s, at : at + 1, :]
             passed = factor * passed + state[s]
             over = over * factor
-        pack_out[target, 0:ch, :] = passed
-        pack_out[target, ch : ch + 8, :] = jnp.broadcast_to(over, (8, ch))
+        folded = passed[0:HEAD_DIM, :]
+        for h in range(1, heads):
+            folded = folded + passed[h * HEAD_DIM : (h + 1) * HEAD_DIM, :]
+        pack_out[target, 0:HEAD_DIM, :] = folded
+        pack_out[target, HEAD_DIM : HEAD_DIM + 8, :] = jnp.broadcast_to(over, (8, ch))
         return inside, reach
 
     ahead_in, ahead_reach = scan_states(state_f, ef, length - 1, range(group), 0)
@@ -659,7 +714,7 @@
         to = own + k * group if way == 0 else own - k * group
         return remote(
             pack_out.at[way], pack_in.at[way, k - 1],
-            pack_send.at[way, k], pack_recv.at[way, k], (to, core),
+            pack_send.at[way, k - 1], pack_recv.at[way, k - 1], (to, core),
         )
 
     def gives(way, k):
@@ -671,8 +726,67 @@
     for k in range(1, planes):
         for way in range(2):
             pl.when(gives(way, k))(lambda way=way, k=k: pack_move(way, k).start())
-    pl.when(middle)(lambda: own_far(CLASS_OUT, 0))
-
+    arrive(CLASS_B, 2, middle)
+    arrive(CLASS_B, 3, middle)
+
+    def feature_cols(kind):
+        return pl.ds(pl.multiple_of(kind * side_rows + place * ch, 128), ch)
+
+    def feature_move(kind, d, s, to):
+        return remote(
+            parts.at[kind, s], feat.at[:, feature_cols(kind)],
+            ft_send.at[0], ft_recv.at[kind, d - 1], (to, core),
+        )
+
+    relay_out(1)
+    arrive(CLASS_OUT, 3, ends)
+    spread_out(3)
+    incoming = []
+    for way in range(2):
+        into[way] = jnp.zeros((HEAD_DIM, ch), f32)
+        into[way + 2] = jnp.ones((HEAD_DIM, ch), f32)
+        for k in range(1, planes):
+            @pl.when(takes(way, k))
+            def _(way=way, k=k):
+                pack_move(way, k).wait_recv()
+                into[way] = into[way] + into[way + 2] * pack_in[way, k - 1, 0:HEAD_DIM, :]
+                into[way + 2] = into[way + 2] * pack_in[
+                    way, k - 1, HEAD_DIM : HEAD_DIM + 1, :
+                ]
+        incoming.append(
+            jnp.where(same_head, jnp.concatenate([into[way]] * heads, axis=0), 0.0)
+        )
+    for s in range(group):
+        state_f[s] = ahead_in[s] + ahead_reach[s] * incoming[0]
+        state_b[s] = back_in[s] + back_reach[s] * incoming[1]
+
+    @pl.loop(0, group)
+    def _(i):
+        d = group - 1 - i
+        s = (lax.rem(lax.rem(place, 2) + lax.rem(d, 2), 2)
+             + 2 * lax.rem(lax.div(place, 2) + lax.div(d, 2), 2))
+        query = rq_buf[s]
+        mix = (
+            loc[s]
+            + ef[s] * jnp.dot(query, state_f[s].astype(bf16), preferred_element_type=f32)
+            + eb[s] * jnp.dot(query, state_b[s].astype(bf16), preferred_element_type=f32)
+        )
+        squares = mix * mix
+        first = jnp.sum(jnp.where(first_head, squares, 0.0), axis=-1, keepdims=True)
+        second = jnp.sum(jnp.where(first_head, 0.0, squares), axis=-1, keepdims=True)
+        scale = lax.rsqrt(jnp.where(first_head, first, second) / HEAD_DIM + EPS)
+        gate = gate_buf[s].astype(f32)
+        parts[1, s] = (
+            gate / (1.0 + jnp.exp(-gate)) * (mix * scale * head_gain_ref[:, place_cols])
+        ).astype(bf16)
+
+        @pl.when(d > 0)
+        def _():
+            feature_move(1, d, s, base + s).start()
+
+    feat[:, feature_cols(1)] = parts[1, place]
+
+    relay_out(2)
     arrive(CLASS_B, 1, ends)
     arrive(CLASS_B, 2, ends)
     pl.when(has_down)(lambda: halos[0].wait_recv())
@@ -692,6 +806,7 @@
             preferred_element_type=f32,
         )
 
+    relay_out(3)
     arrive(CLASS_B, 3, ends)
 
     @pl.loop(0, blocks)
@@ -709,7 +824,7 @@
 
     iv[7:8, :] = iv[all_rows + halo_rows + 7 : all_rows + halo_rows + 8, :]
     iv[all_rows + 8 : all_rows + 9, :] = iv[all_rows + halo_rows + 8 : all_rows + halo_rows + 9, :]
-    own_taps = taps_ref[:, pl.ds(pl.multiple_of(place * ch, 128), ch)]
+    own_taps = taps_ref[:, place_cols]
     for s in range(group):
         at = s * length
         near_sum = (
@@ -719,134 +834,87 @@
         )
         parts[0, s] = (acc[at : at + length, 2 * ch : 3 * ch] * near_sum).astype(bf16)
 
-    def feature_cols(kind):
-        return pl.ds(pl.multiple_of(kind * side_rows + place * ch, 128), ch)
-
-    def feature_move(kind, d, s, to):
-        return remote(
-            parts.at[kind, s], feat.at[:, feature_cols(kind)],
-            ft_send.at[kind, d], ft_recv.at[kind, d], (to, core),
-        )
-
     for d in (3, 1, 2):
         feature_move(0, d, flipped(place, d), chips[d]).start()
     feat[:, feature_cols(0)] = parts[0, place]
 
-    arrive(CLASS_OUT, 1)
-    spread_out(1)
-
-    incoming = []
-    for way in range(2):
-        into[way] = jnp.zeros((ch, ch), f32)
-        into[way + 2] = jnp.ones((ch, ch), f32)
-        for k in range(1, planes):
-            @pl.when(takes(way, k))
-            def _(way=way, k=k):
-                pack_move(way, k).wait_recv()
-                into[way] = into[way] + into[way + 2] * pack_in[way, k - 1, 0:ch, :]
-                into[way + 2] = into[way + 2] * pack_in[way, k - 1, ch : ch + 1, :]
-        incoming.append(into[way])
-    for s in range(group):
-        state_f[s] = ahead_in[s] + ahead_reach[s] * incoming[0]
-        state_b[s] = back_in[s] + back_reach[s] * incoming[1]
-
-    @pl.loop(0, group)
-    def _(i):
-        d = group - 1 - i
-        s = (lax.rem(lax.rem(place, 2) + lax.rem(d, 2), 2)
-             + 2 * lax.rem(lax.div(place, 2) + lax.div(d, 2), 2))
-        query = rq_buf[s]
-        mix = (
-            loc[s]
-            + ef[s] * jnp.dot(query, state_f[s].astype(bf16), preferred_element_type=f32)
-            + eb[s] * jnp.dot(query, state_b[s].astype(bf16), preferred_element_type=f32)
-        )
-        squares = mix * mix
-        first = jnp.sum(jnp.where(first_head, squares, 0.0), axis=-1, keepdims=True)
-        second = jnp.sum(jnp.where(first_head, 0.0, squares), axis=-1, keepdims=True)
-        scale = lax.rsqrt(jnp.where(first_head, first, second) / HEAD_DIM + EPS)
-        gate = gate_buf[s].astype(f32)
-        gain = head_gain_ref[:, pl.ds(pl.multiple_of(place * ch, 128), ch)]
-        parts[1, s] = (gate / (1.0 + jnp.exp(-gate)) * (mix * scale * gain)).astype(bf16)
-
-        @pl.when(d > 0)
-        def _():
-            feature_move(1, d, s, base + s).start()
-
-    feat[:, feature_cols(1)] = parts[1, place]
-
-    relay_out(1)
-    arrive(CLASS_OUT, 2)
-    spread_out(2)
-    relay_out(2)
-    arrive(CLASS_OUT, 3)
-    spread_out(3)
+    my_rows = length // 2
+
+    def part_at(r):
+        return pl.ds(pl.multiple_of(source_plane(r) * part_cols, 128), part_cols)
+
+    def features_here(kind):
+        for d in range(1, group):
+            feature_move(kind, d, flipped(place, d), chips[d]).wait_recv()
+
+    def row_half(c):
+        return pl.ds(pl.multiple_of(c * my_rows, 128), my_rows)
+
+    def share_move(r):
+        return remote(
+            share.at[:, part_at(r)], theirs.at[:, part_at(r)],
+            share_send.at[0], share_recv.at[r], partner,
+        )
+
+    def project(r):
+        def rows_of(c):
+            return (
+                decay[r, 0, row_half(c), :]
+                + jnp.dot(
+                    feat[row_half(c), 0:side_rows], wo[0:side_rows, part_at(r)],
+                    preferred_element_type=f32,
+                )
+            ).astype(bf16)
+
+        share[:, part_at(r)] = rows_of(1 - core)
+        share_move(r).start()
+        out_ref[:, part_at(r)] = rows_of(core)
+
+    def add_theirs(r):
+        share_move(r).wait_recv()
+        out_ref[:, part_at(r)] = (
+            out_ref[:, part_at(r)].astype(f32) + theirs[:, part_at(r)].astype(f32)
+        ).astype(bf16)
+
+    features_here(1)
+    for r in range(planes):
+        finish_out(r)
+        decay[r, 0] = jnp.dot(
+            feat[:, side_rows:], wo[side_rows:, part_at(r)], preferred_element_type=f32
+        )
+    features_here(0)
+    for r in range(planes):
+        project(r)
+    for r in range(planes):
+        add_theirs(r)
+
+    remote(share, theirs, share_send.at[0], share_recv.at[0], partner).wait_send()
     for kind in range(2):
-        for d in (1, 2, 3):
-            feature_move(kind, d, flipped(place, d), chips[d]).wait_recv()
-
-    my_rows = length // 2
-    shares = []
-
-    def project(r):
-        cols = pl.ds(pl.multiple_of(source_plane(r) * part_cols, 128), part_cols)
-
-        def rows_of(c):
-            return jnp.dot(
-                feat[pl.ds(pl.multiple_of(c * my_rows, 128), my_rows), :], wo[:, cols],
-                preferred_element_type=f32,
-            ).astype(bf16)
-
-        share[:, cols] = rows_of(1 - core)
-        move = remote(
-            share.at[:, cols], theirs_ref.at[:, cols], share_send.at[r], share_recv.at[r], partner
-        )
-        move.start()
-        shares.append(move)
-        mine_ref[:, cols] = rows_of(core)
-
-    finish_out(0)
-    project(0)
-    finish_out(1)
-    project(1)
-    relay_out(3)
-    finish_out(2)
-    project(2)
-    finish_out(3)
-    project(3)
-
-    for move in shares:
-        move.wait()
-    for copy in near.values():
-        copy.wait_send()
+        for d in range(1, group):
+            near_block(kind, d).wait_send()
     for copy in rate_moves:
         copy.wait_send()
     ssq_move.wait_send()
-    for copy in tokens.values():
-        copy.wait_send()
-    for d in range(group):
-        halves_block = x.at[span_rows(flipped(place, d)), pl.ds(own_half, half)]
-        remote(halves_block, halves_block, half_send.at[d], half_recv.at[d], partner).wait_send()
-    for r in range(planes):
-        for which, d, hop in ((0, 1, 1), (1, 1, 1), (0, 2, 2), (1, 2, 2), (0, 3, 2), (1, 3, 1)):
-            out_move(r, which, d, hop).wait_send()
+
+    def sent(block, semaphore, landed):
+        remote(block, block, semaphore, landed, partner).wait_send()
+
+    sent(
+        x.at[pl.ds(0, (group - 1) * length), pl.ds(0, 2 * quarter)], tok_send.at[0],
+        tok_recv.at[0, 0],
+    )
+    sent(x.at[pl.ds(0, all_rows), pl.ds(0, half)], half_send.at[0], half_recv.at[0])
+    sent(wo.at[:, pl.ds(0, (group - 1) * planes * out_cols)], wo_send.at[0], wo_recv.at[0, 0, 0])
+    sent(parts.at[:, pl.ds(0, group - 1)], ft_send.at[0], ft_recv.at[0, 0])
     pl.when(has_up)(lambda: halos[0].wait_send())
     pl.when(has_down)(lambda: halos[1].wait_send())
     for k in range(1, planes):
         for way in range(2):
             pl.when(gives(way, k))(lambda way=way, k=k: pack_move(way, k).wait_send())
-    for kind in range(2):
-        for d in range(1, group):
-            feature_move(kind, d, flipped(place, d), chips[d]).wait_send()
     for kind in range(3):
         for q in range(planes):
-            for d in range(places_of(kind)):
-                pl.when(jnp.logical_and(q <= plane, has_up))(
-                    lambda kind=kind, q=q, d=d: far(kind, 0, q, d).wait_send()
-                )
-                pl.when(jnp.logical_and(q >= plane, has_down))(
-                    lambda kind=kind, q=q, d=d: far(kind, 1, q, d).wait_send()
-                )
+            pl.when(jnp.logical_and(q <= plane, has_up))(functools.partial(far_sent, kind, 0, q))
+            pl.when(jnp.logical_and(q >= plane, has_down))(functools.partial(far_sent, kind, 1, q))
 
 
 def turn_tables(spans, length, channels):
@@ -873,44 +941,52 @@
     rows, side = group * length, conv_output.shape[0]
     turn, start = turn_tables(planes * group, length, ch)
     dma = pltpu.SemaphoreType.DMA
-    vmem, anywhere = pl.BlockSpec(memory_space=pltpu.VMEM), pl.BlockSpec(memory_space=pl.ANY)
+    vmem, held = pl.BlockSpec(memory_space=pltpu.VMEM), pl.BlockSpec(memory_space=pltpu.HBM)
     v = pltpu.VMEM
     result = jax.ShapeDtypeStruct((length // 2, width), bf16)
     table = v((group, length, ch), f32)
-    mine, theirs = pl.pallas_call(
+    return pl.pallas_call(
         functools.partial(mixer_kernel, planes, group),
-        out_shape=(result, result),
-        in_specs=[anywhere] * 11 + [vmem] * 5,
-        out_specs=[vmem, vmem],
+        out_shape=result,
+        in_specs=[held] * 16,
+        out_specs=vmem,
         scratch_shapes=[
+            v((1, width), f32), v(conv_taps.shape, f32), v((1, head_gain.shape[0]), f32), v(turn.shape, f32),
+            v((group,) + start.shape[1:], f32),
             v((length, half), bf16), v((rows + 32, width), bf16), v((width, 7 * ch), bf16),
-            v((2 * side, width), bf16), v((group,) + log_decay.shape, f32),
+            v((2 * side, width), bf16), v(log_decay.shape, f32),
+            v((group, 8, length), f32), v((group, 8, length), f32),
             v((8 * group, length), f32), v((128, length), f32),
             v((length, 128), f32), v((length, 128), f32),
             table, table, v((group, heads, length, length), f32),
             table, table, table, table,
             v((group, length, ch), bf16), v((group, length, ch), bf16), v((group, length, ch), bf16),
             table, v((group, ch, ch), f32), v((group, ch, ch), f32),
-            v((2, ch + 8, ch), f32), v((2, planes - 1, ch + 8, ch), f32), v((4, ch, ch), f32),
+            v((2, HEAD_DIM + 8, ch), f32), v((2, planes - 1, HEAD_DIM + 8, ch), f32),
+            v((4, HEAD_DIM, ch), f32),
             v((rows + 32, 3 * ch), f32), v((rows + 48, ch), f32),
             v((2, group, length, ch), bf16), v((length, 2 * side), bf16),
-            v((length // 2, width), bf16),
-            dma((11,)), dma((7, group)), dma((7, group)), dma((group,)), dma((group,)), dma((2,)),
-            dma((2, group)), dma((2, group)), dma((group,)), dma((group,)),
-            dma((3, 2, planes, group)), dma((3, planes, group)),
-            dma((planes, 2, group)), dma((planes, 2, group)), dma((2,)), dma((2,)),
-            dma((2, planes)), dma((2, planes)), dma((2, group)), dma((2, group)),
-            dma((planes,)), dma((planes,)),
+            v((length // 2, width), bf16), v((length // 2, width), bf16),
+            dma((10,)), dma((2, group - 1)), dma((2, group - 1)), dma((1,)), dma((group - 1,)), dma((2,)),
+            dma((1,)), dma((2, group - 1)), dma((1,)), dma((group,)),
+            dma((3, 2, planes)), dma((2, planes, group)), dma((planes,)),
+            dma((1,)), dma((planes, 2, group - 1)), dma((2,)), dma((2,)),
+            dma((2, planes - 1)), dma((2, planes - 1)), dma((1,)), dma((2, group - 1)),
+            dma((1,)), dma((planes,)),
         ],
         compiler_params=pltpu.CompilerParams(
-            collective_id=0, has_side_effects=True, vmem_limit_bytes=60 * 2**20
+            collective_id=0, has_side_effects=True, vmem_limit_bytes=50 * 2**20
         ),
     )(
-        tokens, key_proj, query_proj, value_proj, out_gate, inner_gate, conv_input, outer_gate,
-        conv_output, retention_output, log_decay, norm_gain.reshape(1, -1), conv_taps,
-        head_gain.reshape(1, -1), jnp.asarray(turn), jnp.asarray(start),
-    )
-    return (mine.astype(f32) + theirs.astype(f32)).astype(bf16)
+        *(
+            pltpu.with_memory_space_constraint(source, pltpu.HBM)
+            for source in (
+                tokens, key_proj, query_proj, value_proj, out_gate, inner_gate, conv_input,
+                outer_gate, conv_output, retention_output, log_decay, norm_gain.reshape(1, -1),
+                conv_taps, head_gain.reshape(1, -1), jnp.asarray(turn), jnp.asarray(start),
+            )
+        )
+    )
 
 
 LANES = 128

time: 126 us -> 102 us (0.81)
  Pallas kernels: 122 us -> 101 us
  other arithmetic: 2.91 us -> 0 us
    pallas_call x1, Pallas kernels: 122 us -> 101 us  [mixer(): pl.pallas_call(functools.partial(mixer_kernel, planes, group), out_shape=...]
    convert_element_type x1 -> x0, other arithmetic: 2.91 us -> none  [mixer(): return (mine.astype(f32) + theirs.astype(f32)).astype(bf16)]
where the time goes in v1:
time: 102 us
  Pallas kernels  101 us (99%)
    pallas_call x1, Pallas kernels, mixer(): pl.pallas_call(functools.partial(mixer_kernel, planes, group), out_shape=...  101 us

profile of v1, /device:TPU:0, one launch (start us, length us, event | category | flops | bytes accessed | tf_op | source)
XLA Modules:
  0.0 101.6 jit_solution(6632748074947948658)
XLA Ops:
  0.0 100.7 %shard_map.154 = bf16[256,2048]{1,0:T(8,128)(2,1)S(1)} custom-call(bf16[512,1024]{1,0:T(8,128)(2,1)} %tok_ref.1, bf16[128,512]{1,0:T(8,128)(2,1)} %key_w.1, bf16[128,512]{1,0:T(8,128)(2,1)} %query_w.1, bf16[128,512]{1,0:T(8,128)(2,1)} %value_w.1, bf16[128,512]{1,0:T(8,128)(2,1)} %gate_w.1, bf16[128,512]{1,0:T(8,128)(2,1)} %inner_w.1, ...), custom_call_target="tpu_custom_call" | custom-call | tf_op jit(solution)/shard_map/pallas_call | solution.py:948
  100.7 1.0 copy.18

commit v2 on v1

--- a/solution.py
+++ b/solution.py
@@ -232,10 +232,10 @@
     out_ref, gain_ref, taps_ref, head_gain_ref, turn_ref, base_ref,
     xin, x, w, wo, rate_own, rate_pack, rates, cums, wide, ssq_out, ssq_in, cosines, sines, decay,
     ef, eb, kf, kb, rq_buf, v_buf, gate_buf, loc, state_f, state_b, pack_out, pack_in, into,
-    acc, iv, parts, feat, share, theirs,
+    acc, edges, parts, feat, share, theirs,
     own_sem, near_send, near_recv, rate_send, rate_recv, ssq_sem,
     tok_send, tok_recv, half_send, half_recv, far_send, far_recv, out_recv,
-    wo_send, wo_recv, halo_send, halo_recv, pack_send, pack_recv,
+    wo_send, wo_recv, pair_sem, halo_send, halo_recv, pack_send, pack_recv,
     ft_send, ft_recv, share_send, share_recv,
 ):
     f32, bf16 = jnp.float32, jnp.bfloat16
@@ -338,10 +338,11 @@
         to = flipped(place, d)
         for way in range(2):
             for h in range(heads):
-                rate_pack[d, pl.ds(way * heads + h, 1), :] = rate_own[
-                    way, pl.ds(heads * to + h, 1), :
-                ]
-        rate_pack[d, pl.ds(rate_rows, 8 - rate_rows), :] = jnp.zeros((8 - rate_rows, length), f32)
+                row = rate_own[way, pl.ds(heads * to + h, 1), :]
+                for part in range(2):
+                    rate_pack[d, pl.ds(part * rate_rows + way * heads + h, 1), :] = row[
+                        :, part * length // 2 : (part + 1) * length // 2
+                    ]
     for d in range(1, group):
         rate_moves.append(
             remote(
@@ -444,6 +445,10 @@
             value.astype(bf16)
         )
 
+    def place_at(d):
+        across = lax.rem(lax.rem(place, 2) + lax.rem(d, 2), 2)
+        return across + 2 * lax.rem(lax.div(place, 2) + lax.div(d, 2), 2)
+
     def span_rows(s):
         return pl.ds(pl.multiple_of(s * length, 128), length)
 
@@ -483,7 +488,11 @@
         copy.wait_recv()
     rates[place] = rate_pack[0]
     for s in range(group):
-        cums[s * 8 : s * 8 + 8, :] = rates[s]
+        for part in range(2):
+            cums[s * 8 : s * 8 + rate_rows, part * length // 2 : (part + 1) * length // 2] = rates[
+                s, part * rate_rows : (part + 1) * rate_rows, :
+            ]
+        cums[s * 8 + rate_rows : s * 8 + 8, :] = jnp.zeros((8 - rate_rows, length), f32)
     lanes = lax.broadcasted_iota(jnp.int32, (group * 8, length), 1)
     kinds = lax.rem(lax.broadcasted_iota(jnp.int32, (group * 8, length), 0), 8)
     running = cums[...] * LOG2E
@@ -554,8 +563,12 @@
         out_move(r, 1, 3, 1).start()
 
     def finish_out(r):
-        for which, d in ((1, 1), (0, 2), (0, 3), (1, 3)):
+        for which, d in ((1, 1), (0, 2)) if r == 1 else ((1, 1), (0, 2), (0, 3), (1, 3)):
             out_landed(r, which, d)
+        if r == 1:
+            out_landed(r, 0, 1)
+            out_landed(r, 1, 2)
+            pair_block(source_plane(1)).wait_recv()
 
     def wait_half(d):
         block = x.at[
@@ -647,16 +660,23 @@
             target[s] = jnp.where(same_head, state, 0.0)
 
     halo_rows = 16
-    halos = [
-        remote(
-            x.at[pl.ds(all_rows - halo_rows, halo_rows), :], x.at[pl.ds(all_rows, halo_rows), :],
-            halo_send.at[0], halo_recv.at[0], (own + group, core),
-        ),
-        remote(
-            x.at[pl.ds(0, halo_rows), :], x.at[pl.ds(all_rows + halo_rows, halo_rows), :],
-            halo_send.at[1], halo_recv.at[1], (own - group, core),
-        ),
-    ]
+    halo_at = (all_rows, all_rows + halo_rows)
+
+    def halo_move(way):
+        cols = pl.ds(own_half, half)
+        source = x.at[pl.ds((all_rows - halo_rows) * (1 - way), halo_rows), cols]
+        return remote(
+            source, x.at[pl.ds(halo_at[way], halo_rows), cols],
+            halo_send.at[way], halo_recv.at[way], (own + group if way == 0 else own - group, core),
+        )
+
+    def halo_pass(way):
+        block = x.at[pl.ds(halo_at[way], halo_rows), pl.ds(own_half, half)]
+        return remote(block, block, halo_send.at[2 + way], halo_recv.at[2 + way], partner)
+
+    def halo_comes(way):
+        return has_down if way == 0 else has_up
+
     blank = jnp.zeros((halo_rows, width), bf16)
 
     @pl.when(jnp.logical_not(has_down))
@@ -683,14 +703,13 @@
         @pl.when(d == 3)
         def _():
             wait_half(3)
-            pl.when(has_up)(lambda: halos[0].start())
-            pl.when(has_down)(lambda: halos[1].start())
+            pl.when(has_up)(lambda: halo_move(0).start())
+            pl.when(has_down)(lambda: halo_move(1).start())
             relay_out(0)
             arrive(CLASS_OUT, 2, ends)
             spread_out(2)
 
-        one_span(lax.rem(lax.rem(place, 2) + lax.rem(d, 2), 2)
-                 + 2 * lax.rem(lax.div(place, 2) + lax.div(d, 2), 2))
+        one_span(place_at(d))
 
     def scan_states(state, table, at, order, target):
         passed, inside, reach = jnp.zeros((ch, ch), f32), {}, {}
@@ -738,7 +757,17 @@
             ft_send.at[0], ft_recv.at[kind, d - 1], (to, core),
         )
 
-    relay_out(1)
+    finish_out(0)
+
+    def pair_block(q):
+        start = pl.multiple_of((q * group + flipped(place, 3)) * out_cols, 128)
+        block = wo.at[:, pl.ds(start, out_cols)]
+        return remote(
+            block, block, pair_sem.at[0], pair_sem.at[1],
+            ((plane + 1 - 2 * lax.rem(plane, 2)) * group + place, core),
+        )
+
+    pair_block(plane).start()
     arrive(CLASS_OUT, 3, ends)
     spread_out(3)
     incoming = []
@@ -763,8 +792,7 @@
     @pl.loop(0, group)
     def _(i):
         d = group - 1 - i
-        s = (lax.rem(lax.rem(place, 2) + lax.rem(d, 2), 2)
-             + 2 * lax.rem(lax.div(place, 2) + lax.div(d, 2), 2))
+        s = place_at(d)
         query = rq_buf[s]
         mix = (
             loc[s]
@@ -786,11 +814,16 @@
 
     feat[:, feature_cols(1)] = parts[1, place]
 
+    for way in range(2):
+        @pl.when(halo_comes(way))
+        def _(way=way):
+            halo_move(way).wait_recv()
+            halo_pass(way).start()
     relay_out(2)
     arrive(CLASS_B, 1, ends)
     arrive(CLASS_B, 2, ends)
-    pl.when(has_down)(lambda: halos[0].wait_recv())
-    pl.when(has_up)(lambda: halos[1].wait_recv())
+    for way in range(2):
+        pl.when(halo_comes(way))(lambda way=way: halo_pass(way).wait_recv())
     depth = group * rows_in
     most = (planes - 1) * depth
     early = pl.multiple_of(top * depth, 128)
@@ -809,33 +842,53 @@
     relay_out(3)
     arrive(CLASS_B, 3, ends)
 
-    @pl.loop(0, blocks)
-    def _(t):
-        rows = pl.ds(pl.multiple_of(t * block, 16), block)
+    spans_at = [s * length - halo_rows for s in range(1, group)] + [all_rows]
+    late_w = w[pl.ds(late, depth), col_a : col_a + col_b]
+    near_rows = jnp.concatenate(
+        [x[at : at + 2 * halo_rows, pl.ds(late, depth)] for at in spans_at], axis=0
+    )
+    near_sums = jnp.concatenate(
+        [acc[at : at + 2 * halo_rows, 0 : 2 * ch] for at in spans_at], axis=0
+    )
+
+    def inner_product(held):
+        held = held.astype(bf16).astype(f32)
+        return (held[:, 0:ch] * held[:, ch : 2 * ch]).astype(bf16).astype(f32)
+
+    edge_values = inner_product(
+        near_sums + jnp.dot(near_rows, late_w[:, 0 : 2 * ch], preferred_element_type=f32)
+    )
+    for s in range(group):
+        before = ((s - 1) % group) * 2 * halo_rows + halo_rows - 1
+        after = s * 2 * halo_rows + halo_rows
+        edges[s, 0:1, :] = edge_values[before : before + 1, :]
+        edges[s, 1:2, :] = edge_values[after : after + 1, :]
+    row_of = lax.broadcasted_iota(jnp.int32, (length, ch), 0)
+
+    @pl.loop(0, group)
+    def _(i):
+        turned_round = lax.div(i, 2)
+        d = (1 - turned_round) * (1 + 2 * i) + turned_round * (6 - 2 * i)
+        s = place_at(d)
+        rows = span_rows(s)
         held = acc[rows, :] + jnp.dot(
             x[rows, pl.ds(late, depth)], w[pl.ds(late, depth), col_a : col_a + col_b],
             preferred_element_type=f32,
         )
-        held = held.astype(bf16).astype(f32)
-        iv[pl.ds(pl.multiple_of(t * block + 8, 8), block), :] = (
-            (held[:, 0:ch] * held[:, ch : 2 * ch]).astype(bf16).astype(f32)
-        )
-        acc[rows, 2 * ch : 3 * ch] = held[:, 2 * ch : 3 * ch]
-
-    iv[7:8, :] = iv[all_rows + halo_rows + 7 : all_rows + halo_rows + 8, :]
-    iv[all_rows + 8 : all_rows + 9, :] = iv[all_rows + halo_rows + 8 : all_rows + halo_rows + 9, :]
-    own_taps = taps_ref[:, place_cols]
-    for s in range(group):
-        at = s * length
+        inner = inner_product(held)
+        before = jnp.where(row_of == 0, edges[s, 0:1, :], pltpu.roll(inner, 1, 0))
+        after = jnp.where(row_of == length - 1, edges[s, 1:2, :], pltpu.roll(inner, length - 1, 0))
         near_sum = (
-            own_taps[0:1, :] * iv[at + 7 : at + 7 + length, :]
-            + own_taps[1:2, :] * iv[at + 8 : at + 8 + length, :]
-            + own_taps[2:3, :] * iv[at + 9 : at + 9 + length, :]
-        )
-        parts[0, s] = (acc[at : at + length, 2 * ch : 3 * ch] * near_sum).astype(bf16)
-
-    for d in (3, 1, 2):
-        feature_move(0, d, flipped(place, d), chips[d]).start()
+            taps_ref[0:1, place_cols] * before
+            + taps_ref[1:2, place_cols] * inner
+            + taps_ref[2:3, place_cols] * after
+        )
+        parts[0, s] = (held[:, 2 * ch : 3 * ch].astype(bf16).astype(f32) * near_sum).astype(bf16)
+
+        @pl.when(d > 0)
+        def _():
+            feature_move(0, d, s, base + s).start()
+
     feat[:, feature_cols(0)] = parts[0, place]
 
     my_rows = length // 2
@@ -843,8 +896,8 @@
     def part_at(r):
         return pl.ds(pl.multiple_of(source_plane(r) * part_cols, 128), part_cols)
 
-    def features_here(kind):
-        for d in range(1, group):
+    def features_here(kind, places=(1, 2, 3)):
+        for d in places:
             feature_move(kind, d, flipped(place, d), chips[d]).wait_recv()
 
     def row_half(c):
@@ -856,19 +909,16 @@
             share_send.at[0], share_recv.at[r], partner,
         )
 
-    def project(r):
-        def rows_of(c):
-            return (
-                decay[r, 0, row_half(c), :]
-                + jnp.dot(
-                    feat[row_half(c), 0:side_rows], wo[0:side_rows, part_at(r)],
-                    preferred_element_type=f32,
-                )
-            ).astype(bf16)
-
-        share[:, part_at(r)] = rows_of(1 - core)
-        share_move(r).start()
-        out_ref[:, part_at(r)] = rows_of(core)
+    pair_rows = 2 * ch
+    own_pair = lax.div(place, 2)
+
+    def conv_part(c, r, pair):
+        at = pl.ds(pl.multiple_of(pair * pair_rows, 128), pair_rows)
+        rows = pl.ds(0, length) if c is None else row_half(c)
+        return jnp.dot(feat[rows, at], wo[at, part_at(r)], preferred_element_type=f32)
+
+    def rows_of(c, r):
+        return (decay[r, 0, row_half(c), :] + conv_part(c, r, 1 - own_pair)).astype(bf16)
 
     def add_theirs(r):
         share_move(r).wait_recv()
@@ -878,17 +928,11 @@
 
     features_here(1)
     for r in range(planes):
-        finish_out(r)
+        if r > 0:
+            finish_out(r)
         decay[r, 0] = jnp.dot(
             feat[:, side_rows:], wo[side_rows:, part_at(r)], preferred_element_type=f32
         )
-    features_here(0)
-    for r in range(planes):
-        project(r)
-    for r in range(planes):
-        add_theirs(r)
-
-    remote(share, theirs, share_send.at[0], share_recv.at[0], partner).wait_send()
     for kind in range(2):
         for d in range(1, group):
             near_block(kind, d).wait_send()
@@ -904,10 +948,12 @@
         tok_recv.at[0, 0],
     )
     sent(x.at[pl.ds(0, all_rows), pl.ds(0, half)], half_send.at[0], half_recv.at[0])
-    sent(wo.at[:, pl.ds(0, (group - 1) * planes * out_cols)], wo_send.at[0], wo_recv.at[0, 0, 0])
-    sent(parts.at[:, pl.ds(0, group - 1)], ft_send.at[0], ft_recv.at[0, 0])
-    pl.when(has_up)(lambda: halos[0].wait_send())
-    pl.when(has_down)(lambda: halos[1].wait_send())
+    sent(wo.at[:, pl.ds(0, ((group - 1) * planes - 1) * out_cols)], wo_send.at[0], wo_recv.at[0, 0, 0])
+    pair_block(plane).wait_send()
+    pl.when(has_up)(lambda: halo_move(0).wait_send())
+    pl.when(has_down)(lambda: halo_move(1).wait_send())
+    for way in range(2):
+        pl.when(halo_comes(way))(lambda way=way: halo_pass(way).wait_send())
     for k in range(1, planes):
         for way in range(2):
             pl.when(gives(way, k))(lambda way=way, k=k: pack_move(way, k).wait_send())
@@ -915,6 +961,20 @@
         for q in range(planes):
             pl.when(jnp.logical_and(q <= plane, has_up))(functools.partial(far_sent, kind, 0, q))
             pl.when(jnp.logical_and(q >= plane, has_down))(functools.partial(far_sent, kind, 1, q))
+
+    features_here(0, (1,))
+    for r in range(planes):
+        decay[r, 0] = decay[r, 0] + conv_part(None, r, own_pair)
+    features_here(0, (2, 3))
+    for r in range(planes):
+        share[:, part_at(r)] = rows_of(1 - core, r)
+        share_move(r).start()
+    for r in range(planes):
+        out_ref[:, part_at(r)] = rows_of(core, r)
+    for r in range(planes):
+        add_theirs(r)
+    remote(share, theirs, share_send.at[0], share_recv.at[0], partner).wait_send()
+    sent(parts.at[:, pl.ds(0, group - 1)], ft_send.at[0], ft_recv.at[0, 0])
 
 
 def turn_tables(spans, length, channels):
@@ -955,7 +1015,7 @@
             v((group,) + start.shape[1:], f32),
             v((length, half), bf16), v((rows + 32, width), bf16), v((width, 7 * ch), bf16),
             v((2 * side, width), bf16), v(log_decay.shape, f32),
-            v((group, 8, length), f32), v((group, 8, length), f32),
+            v((group, 4 * heads, length // 2), f32), v((group, 4 * heads, length // 2), f32),
             v((8 * group, length), f32), v((128, length), f32),
             v((length, 128), f32), v((length, 128), f32),
             table, table, v((group, heads, length, length), f32),
@@ -964,13 +1024,13 @@
             table, v((group, ch, ch), f32), v((group, ch, ch), f32),
             v((2, HEAD_DIM + 8, ch), f32), v((2, planes - 1, HEAD_DIM + 8, ch), f32),
             v((4, HEAD_DIM, ch), f32),
-            v((rows + 32, 3 * ch), f32), v((rows + 48, ch), f32),
+            v((rows + 32, 3 * ch), f32), v((group, 8, ch), f32),
             v((2, group, length, ch), bf16), v((length, 2 * side), bf16),
             v((length // 2, width), bf16), v((length // 2, width), bf16),
             dma((10,)), dma((2, group - 1)), dma((2, group - 1)), dma((1,)), dma((group - 1,)), dma((2,)),
             dma((1,)), dma((2, group - 1)), dma((1,)), dma((group,)),
             dma((3, 2, planes)), dma((2, planes, group)), dma((planes,)),
-            dma((1,)), dma((planes, 2, group - 1)), dma((2,)), dma((2,)),
+            dma((1,)), dma((planes, 2, group - 1)), dma((2,)), dma((4,)), dma((4,)),
             dma((2, planes - 1)), dma((2, planes - 1)), dma((1,)), dma((2, group - 1)),
             dma((1,)), dma((planes,)),
         ],

time: 102 us -> 99.3 us (0.974)
  Pallas kernels: 101 us -> 98.2 us
    pallas_call x1, Pallas kernels: 101 us -> 98.2 us  [mixer(): pl.pallas_call(functools.partial(mixer_kernel, planes, group), out_shape=...]
where the time goes in v2:
time: 99.3 us; the launch traced here: 99.2 us
  Pallas kernels  98.2 us (99%)
    pallas_call x1, Pallas kernels, mixer(): pl.pallas_call(functools.partial(mixer_kernel, planes, group), out_shape=...  98.2 us

profile of v2, /device:TPU:0, one launch (start us, length us, event | category | flops | bytes accessed | tf_op | source)
XLA Modules:
  0.0 99.2 jit_solution(15052857798481174999)
XLA Ops:
  0.0 98.2 %shard_map.154 = bf16[256,2048]{1,0:T(8,128)(2,1)S(1)} custom-call(bf16[512,1024]{1,0:T(8,128)(2,1)} %tok_ref.1, bf16[128,512]{1,0:T(8,128)(2,1)} %key_w.1, bf16[128,512]{1,0:T(8,128)(2,1)} %query_w.1, bf16[128,512]{1,0:T(8,128)(2,1)} %value_w.1, bf16[128,512]{1,0:T(8,128)(2,1)} %gate_w.1, bf16[128,512]{1,0:T(8,128)(2,1)} %inner_w.1, ...), custom_call_target="tpu_custom_call" | custom-call | tf_op jit(solution)/shard_map/pallas_call | solution.py:1008
  98.2 1.0 copy.18

commit v3 on v2

--- a/solution.py
+++ b/solution.py
@@ -232,11 +232,11 @@
     out_ref, gain_ref, taps_ref, head_gain_ref, turn_ref, base_ref,
     xin, x, w, wo, rate_own, rate_pack, rates, cums, wide, ssq_out, ssq_in, cosines, sines, decay,
     ef, eb, kf, kb, rq_buf, v_buf, gate_buf, loc, state_f, state_b, pack_out, pack_in, into,
-    acc, edges, parts, feat, share, theirs,
+    acc, edges, parts, feat,
     own_sem, near_send, near_recv, rate_send, rate_recv, ssq_sem,
     tok_send, tok_recv, half_send, half_recv, far_send, far_recv, out_recv,
-    wo_send, wo_recv, pair_sem, halo_send, halo_recv, pack_send, pack_recv,
-    ft_send, ft_recv, share_send, share_recv,
+    wo_send, wo_recv, mate_send, mate_recv, pair_sem, halo_send, halo_recv, pack_send, pack_recv,
+    ft_send, ft_recv,
 ):
     f32, bf16 = jnp.float32, jnp.bfloat16
     own, core = lax.axis_index("sp"), lax.axis_index("tp")
@@ -280,8 +280,8 @@
                 w.at[own_rows, pl.ds(j * ch, ch)], 2 + j // 4,
             )
         )
-    kept.append(local_copy(cout_ref, wo.at[pl.ds(0, side_rows), own_cols], 4))
-    kept.append(local_copy(rout_ref, wo.at[pl.ds(side_rows, side_rows), own_cols], 4))
+    kept.append(local_copy(cout_ref, wo.at[core, pl.ds(0, side_rows), own_cols], 4))
+    kept.append(local_copy(rout_ref, wo.at[core, pl.ds(side_rows, side_rows), own_cols], 4))
     place_cols = pl.ds(pl.multiple_of(place * ch, 128), ch)
     small = [
         local_copy(gain_in, gain_ref, 5),
@@ -297,7 +297,7 @@
         return pl.ds(0, col_a) if kind == CLASS_A else pl.ds(col_a, col_b)
 
     def own_here(kind):
-        block = wo.at[:, own_cols] if kind == CLASS_OUT else w.at[own_rows, class_cols(kind)]
+        block = wo.at[core, :, own_cols] if kind == CLASS_OUT else w.at[own_rows, class_cols(kind)]
         local_copy(block, block, 2 + kind).wait()
 
     barrier = pltpu.get_barrier_semaphore()
@@ -306,25 +306,26 @@
         pl.semaphore_signal(barrier, inc=1, device_id=target, device_id_type=mesh_id)
 
     for d in range(1, group):
-        greet((chips[d], core))
+        for c in range(2):
+            greet((chips[d], c))
     greet(partner)
     for k in range(1, planes):
         greet((lax.rem(own + k * group, planes * group), core))
-    pl.semaphore_wait(barrier, group + planes - 1)
+    pl.semaphore_wait(barrier, 2 * group + planes - 2)
 
     def send_near(j, d):
         to = flipped(place, d)
         remote(
             weights[j].at[:, pl.ds(pl.multiple_of(to * ch, 128), ch)],
             w.at[own_rows, pl.ds(j * ch, ch)],
-            near_send.at[j // 4, d - 1], near_recv.at[j // 4, d - 1], (chips[d], core),
+            near_send.at[0], near_recv.at[j // 4, d - 1], (chips[d], core),
         ).start()
 
     def near_block(kind, d):
         start = pl.multiple_of((base + flipped(place, d)) * rows_in, 128)
         block = w.at[pl.ds(start, rows_in), class_cols(kind)]
         return remote(
-            block, block, near_send.at[kind, d - 1], near_recv.at[kind, d - 1], (chips[d], core)
+            block, block, near_send.at[0], near_recv.at[kind, d - 1], (chips[d], core)
         )
 
     for d in range(1, group):
@@ -358,25 +359,41 @@
 
     def far(kind, direction, q, d):
         if kind == CLASS_OUT:
-            block = wo.at[:, pl.ds(pl.multiple_of((q * group + place) * out_cols, 128), out_cols)]
+            block = wo.at[
+                core, :, pl.ds(pl.multiple_of((q * group + place) * out_cols, 128), out_cols)
+            ]
         else:
             start = pl.multiple_of((q * group + flipped(place, d)) * rows_in, 128)
             block = w.at[pl.ds(start, rows_in), class_cols(kind)]
-        landed = out_recv.at[q] if kind == CLASS_OUT else far_recv.at[kind, q, d]
-        target = own + group if direction == 0 else own - group
-        return remote(block, block, far_send.at[kind, direction, q], landed, (target, core))
-
-    def far_sent(kind, direction, q):
+        to = plane + 1 - 2 * direction
+        return remote(
+            block, block, far_send.at[kind, direction], far_landed(kind, q, d, to),
+            (own + group * (1 - 2 * direction), core),
+        )
+
+    def far_landed(kind, q, d, at):
+        slot = q - (q > at).astype(jnp.int32)
+        return out_recv.at[slot] if kind == CLASS_OUT else far_recv.at[kind, slot, d]
+
+    def far_arrived(kind, q, d):
         if kind == CLASS_OUT:
-            far(kind, direction, q, 0).wait_send()
+            block = wo.at[
+                core, :, pl.ds(pl.multiple_of((q * group + place) * out_cols, 128), out_cols)
+            ]
         else:
-            block = w.at[
-                pl.ds(pl.multiple_of(q * group * rows_in, 128), group * rows_in), class_cols(kind)
-            ]
-            remote(
-                block, block, far_send.at[kind, direction, q], far_recv.at[kind, q, 0],
-                (own + group, core),
-            ).wait_send()
+            start = pl.multiple_of((q * group + flipped(place, d)) * rows_in, 128)
+            block = w.at[pl.ds(start, rows_in), class_cols(kind)]
+        remote(
+            block, block, far_send.at[kind, 0], far_landed(kind, q, d, plane), partner
+        ).wait_recv()
+
+    def far_sent(kind, direction, units):
+        if kind == CLASS_OUT:
+            block, landed = wo.at[core, :, pl.ds(0, units * out_cols)], out_recv.at[0]
+        else:
+            block = w.at[pl.ds(0, units * group * rows_in), class_cols(kind)]
+            landed = far_recv.at[kind, 0, 0]
+        remote(block, block, far_send.at[kind, direction], landed, partner).wait_send()
 
     def places_of(kind):
         return 1 if kind == CLASS_OUT else group
@@ -397,7 +414,7 @@
 
         def take():
             for d in range(places_of(kind)) if blocks is None else blocks:
-                far(kind, 0, q, d).wait_recv()
+                far_arrived(kind, q, d)
                 pl.when(jnp.logical_and(q < plane, has_up))(
                     lambda d=d: far(kind, 0, q, d).start()
                 )
@@ -460,11 +477,14 @@
 
     tokens = {}
 
+    def token_landed(which, d):
+        return tok_recv.at[4] if d == 3 else tok_recv.at[which * 2 + d - 1]
+
     def send_piece(which, d_from, hop):
         d_there = d_from + hop
         tokens[(which, d_there)] = remote(
             piece(d_from, which), piece(d_from, which),
-            tok_send.at[0], tok_recv.at[which, d_there - 1], (chips[hop], core),
+            tok_send.at[0], token_landed(which, d_there), (chips[hop], core),
         )
         tokens[(which, d_there)].start()
 
@@ -537,20 +557,22 @@
 
     def out_piece(r, d, which):
         start = pl.multiple_of((source_plane(r) * group + flipped(place, d)) * out_cols, 128)
-        return wo.at[pl.ds(which * side_rows, side_rows), pl.ds(start, out_cols)]
+        return wo.at[core, pl.ds(which * side_rows, side_rows), pl.ds(start, out_cols)]
 
     def out_move(r, which, d_there, hop):
         block = out_piece(r, d_there - hop, which)
         return remote(
-            block, block, wo_send.at[0], wo_recv.at[r, which, d_there - 1],
+            block, block, wo_send.at[0], out_sem(r, which, d_there),
             (chips[hop], core),
         )
+
+    def out_sem(r, which, d):
+        first = (which, d) == (0, 1)
+        return wo_recv.at[r, 0 if first else 1 if (which, d) == (1, 2) else 2]
 
     def out_landed(r, which, d):
         block = out_piece(r, d, which)
-        remote(
-            block, block, wo_send.at[0], wo_recv.at[r, which, d - 1], (chips[1], core)
-        ).wait_recv()
+        remote(block, block, wo_send.at[0], out_sem(r, which, d), partner).wait_recv()
 
     def spread_out(r):
         for which, hop in ((0, 1), (1, 2), (1, 1), (0, 2)):
@@ -563,12 +585,27 @@
         out_move(r, 1, 3, 1).start()
 
     def finish_out(r):
-        for which, d in ((1, 1), (0, 2)) if r == 1 else ((1, 1), (0, 2), (0, 3), (1, 3)):
-            out_landed(r, which, d)
+        pieces = 1 if r == 1 else 2
+        block = wo.at[core, :, pl.ds(0, pieces * out_cols)]
+        remote(block, block, wo_send.at[0], wo_recv.at[r, 2], partner).wait_recv()
         if r == 1:
             out_landed(r, 0, 1)
             out_landed(r, 1, 2)
-            pair_block(source_plane(1)).wait_recv()
+
+    def part_at(r):
+        return pl.ds(pl.multiple_of(source_plane(r) * part_cols, 128), part_cols)
+
+    def out_block(r, d):
+        start = pl.multiple_of((source_plane(r) * group + flipped(place, d)) * out_cols, 128)
+        return pl.ds(start, out_cols)
+
+    def mate_copy(cols, i):
+        block = wo.at[core, :, cols]
+        return remote(block, block, mate_send.at[0], mate_recv.at[i], partner)
+
+    def mate_here(cols, i):
+        block = wo.at[1 - core, :, cols]
+        remote(block, block, mate_send.at[0], mate_recv.at[i], partner).wait_recv()
 
     def wait_half(d):
         block = x.at[
@@ -691,8 +728,10 @@
     def _(d):
         @pl.when(d == 1)
         def _():
-            tokens[(0, 3)].wait_recv()
-            tokens[(1, 3)].wait_recv()
+            last = x.at[
+                span_rows(flipped(place, 3)), pl.ds(pl.multiple_of(core * half, 128), half)
+            ]
+            remote(last, last, tok_send.at[0], token_landed(0, 3), partner).wait_recv()
             send_half(3)
             wait_half(1)
 
@@ -751,23 +790,40 @@
     def feature_cols(kind):
         return pl.ds(pl.multiple_of(kind * side_rows + place * ch, 128), ch)
 
-    def feature_move(kind, d, s, to):
+    my_rows = length // 2
+
+    def row_half(c):
+        return pl.ds(pl.multiple_of(c * my_rows, 128), my_rows)
+
+    def feature_move(kind, d, s, c):
+        sender = ft_send.at[0]
         return remote(
-            parts.at[kind, s], feat.at[:, feature_cols(kind)],
-            ft_send.at[0], ft_recv.at[kind, d - 1], (to, core),
-        )
+            parts.at[kind, s, row_half(c)], feat.at[core, :, feature_cols(kind)],
+            sender, ft_recv.at[kind, d], (base + s, c),
+        )
+
+    def feature_mate(kind):
+        return remote(
+            parts.at[kind, place, row_half(1 - core)], feat.at[core, :, feature_cols(kind)],
+            ft_send.at[1], ft_recv.at[kind, 0], partner,
+        )
+
+    def own_features(kind):
+        feature_mate(kind).start()
+        feat[core, :, feature_cols(kind)] = parts[kind, place, row_half(core), :]
 
     finish_out(0)
 
     def pair_block(q):
         start = pl.multiple_of((q * group + flipped(place, 3)) * out_cols, 128)
-        block = wo.at[:, pl.ds(start, out_cols)]
+        block = wo.at[core, :, pl.ds(start, out_cols)]
         return remote(
             block, block, pair_sem.at[0], pair_sem.at[1],
             ((plane + 1 - 2 * lax.rem(plane, 2)) * group + place, core),
         )
 
     pair_block(plane).start()
+    mate_copy(part_at(0), 0).start()
     arrive(CLASS_OUT, 3, ends)
     spread_out(3)
     incoming = []
@@ -810,9 +866,10 @@
 
         @pl.when(d > 0)
         def _():
-            feature_move(1, d, s, base + s).start()
-
-    feat[:, feature_cols(1)] = parts[1, place]
+            for c in range(2):
+                feature_move(1, d, s, c).start()
+
+    own_features(1)
 
     for way in range(2):
         @pl.when(halo_comes(way))
@@ -840,6 +897,9 @@
         )
 
     relay_out(3)
+    finish_out(1)
+    for d in range(group - 1):
+        mate_copy(out_block(1, d), 1).start()
     arrive(CLASS_B, 3, ends)
 
     spans_at = [s * length - halo_rows for s in range(1, group)] + [all_rows]
@@ -887,55 +947,55 @@
 
         @pl.when(d > 0)
         def _():
-            feature_move(0, d, s, base + s).start()
-
-    feat[:, feature_cols(0)] = parts[0, place]
-
-    my_rows = length // 2
-
-    def part_at(r):
-        return pl.ds(pl.multiple_of(source_plane(r) * part_cols, 128), part_cols)
-
-    def features_here(kind, places=(1, 2, 3)):
+            for c in range(2):
+                feature_move(0, d, s, c).start()
+
+    own_features(0)
+
+    def features_here(kind, places):
         for d in places:
-            feature_move(kind, d, flipped(place, d), chips[d]).wait_recv()
-
-    def row_half(c):
-        return pl.ds(pl.multiple_of(c * my_rows, 128), my_rows)
-
-    def share_move(r):
-        return remote(
-            share.at[:, part_at(r)], theirs.at[:, part_at(r)],
-            share_send.at[0], share_recv.at[r], partner,
-        )
+            rows = my_rows if d == 0 else length
+            block = parts.at[0, 0, pl.ds(0, rows)]
+            remote(block, block, ft_send.at[0], ft_recv.at[kind, d], partner).wait_recv()
+
+    def product(rows, r):
+        total = None
+        for c in range(2):
+            part = jnp.dot(feat[c, :, rows], wo[c, rows, part_at(r)], preferred_element_type=f32)
+            total = part if total is None else total + part
+        return total
+
+    def retention_product(r):
+        decay[r, 0, 0:my_rows, :] = product(pl.ds(side_rows, side_rows), r)
 
     pair_rows = 2 * ch
     own_pair = lax.div(place, 2)
 
-    def conv_part(c, r, pair):
+    def conv_product(r, pair):
         at = pl.ds(pl.multiple_of(pair * pair_rows, 128), pair_rows)
-        rows = pl.ds(0, length) if c is None else row_half(c)
-        return jnp.dot(feat[rows, at], wo[at, part_at(r)], preferred_element_type=f32)
-
-    def rows_of(c, r):
-        return (decay[r, 0, row_half(c), :] + conv_part(c, r, 1 - own_pair)).astype(bf16)
-
-    def add_theirs(r):
-        share_move(r).wait_recv()
-        out_ref[:, part_at(r)] = (
-            out_ref[:, part_at(r)].astype(f32) + theirs[:, part_at(r)].astype(f32)
-        ).astype(bf16)
-
-    features_here(1)
-    for r in range(planes):
-        if r > 0:
-            finish_out(r)
-        decay[r, 0] = jnp.dot(
-            feat[:, side_rows:], wo[side_rows:, part_at(r)], preferred_element_type=f32
-        )
-    for kind in range(2):
-        for d in range(1, group):
-            near_block(kind, d).wait_send()
+        return decay[r, 0, 0:my_rows, :] + product(at, r)
+
+    features_here(1, range(group))
+    mate_here(part_at(0), 0)
+    retention_product(0)
+    finish_out(2)
+    mate_copy(part_at(2), 3).start()
+    finish_out(3)
+    mate_copy(part_at(3), 4).start()
+    mate_here(part_at(2), 3)
+    retention_product(2)
+    pair_block(source_plane(1)).wait_recv()
+    mate_copy(out_block(1, 3), 2).start()
+    mate_here(part_at(3), 4)
+    retention_product(3)
+    features_here(0, (0, 1))
+    for r in (0, 2, 3):
+        decay[r, 0, 0:my_rows, :] = conv_product(r, own_pair)
+    mate_here(pl.ds(0, (group - 1) * out_cols), 1)
+    mate_here(out_block(1, 3), 2)
+    retention_product(1)
+    decay[1, 0, 0:my_rows, :] = conv_product(1, own_pair)
+
     for copy in rate_moves:
         copy.wait_send()
     ssq_move.wait_send()
@@ -945,11 +1005,18 @@
 
     sent(
         x.at[pl.ds(0, (group - 1) * length), pl.ds(0, 2 * quarter)], tok_send.at[0],
-        tok_recv.at[0, 0],
+        tok_recv.at[0],
     )
     sent(x.at[pl.ds(0, all_rows), pl.ds(0, half)], half_send.at[0], half_recv.at[0])
-    sent(wo.at[:, pl.ds(0, ((group - 1) * planes - 1) * out_cols)], wo_send.at[0], wo_recv.at[0, 0, 0])
+    sent(
+        wo.at[core, :, pl.ds(0, ((group - 1) * planes - 1) * out_cols)], wo_send.at[0],
+        wo_recv.at[0, 0],
+    )
     pair_block(plane).wait_send()
+    sent(
+        w.at[pl.ds(0, (group - 1) * rows_in), :], near_send.at[0], near_recv.at[0, 0]
+    )
+    sent(wo.at[core], mate_send.at[0], mate_recv.at[0])
     pl.when(has_up)(lambda: halo_move(0).wait_send())
     pl.when(has_down)(lambda: halo_move(1).wait_send())
     for way in range(2):
@@ -958,23 +1025,15 @@
         for way in range(2):
             pl.when(gives(way, k))(lambda way=way, k=k: pack_move(way, k).wait_send())
     for kind in range(3):
-        for q in range(planes):
-            pl.when(jnp.logical_and(q <= plane, has_up))(functools.partial(far_sent, kind, 0, q))
-            pl.when(jnp.logical_and(q >= plane, has_down))(functools.partial(far_sent, kind, 1, q))
-
-    features_here(0, (1,))
-    for r in range(planes):
-        decay[r, 0] = decay[r, 0] + conv_part(None, r, own_pair)
+        for units in range(1, planes):
+            pl.when(plane == units - 1)(functools.partial(far_sent, kind, 0, units))
+            pl.when(plane == planes - units)(functools.partial(far_sent, kind, 1, units))
+
     features_here(0, (2, 3))
     for r in range(planes):
-        share[:, part_at(r)] = rows_of(1 - core, r)
-        share_move(r).start()
-    for r in range(planes):
-        out_ref[:, part_at(r)] = rows_of(core, r)
-    for r in range(planes):
-        add_theirs(r)
-    remote(share, theirs, share_send.at[0], share_recv.at[0], partner).wait_send()
+        out_ref[:, part_at(r)] = conv_product(r, 1 - own_pair).astype(bf16)
     sent(parts.at[:, pl.ds(0, group - 1)], ft_send.at[0], ft_recv.at[0, 0])
+    sent(parts.at[:, 0, pl.ds(0, my_rows)], ft_send.at[1], ft_recv.at[0, 0])
 
 
 def turn_tables(spans, length, channels):
@@ -1014,7 +1073,7 @@
             v((1, width), f32), v(conv_taps.shape, f32), v((1, head_gain.shape[0]), f32), v(turn.shape, f32),
             v((group,) + start.shape[1:], f32),
             v((length, half), bf16), v((rows + 32, width), bf16), v((width, 7 * ch), bf16),
-            v((2 * side, width), bf16), v(log_decay.shape, f32),
+            v((2, 2 * side, width), bf16), v(log_decay.shape, f32),
             v((group, 4 * heads, length // 2), f32), v((group, 4 * heads, length // 2), f32),
             v((8 * group, length), f32), v((128, length), f32),
             v((length, 128), f32), v((length, 128), f32),
@@ -1025,14 +1084,12 @@
             v((2, HEAD_DIM + 8, ch), f32), v((2, planes - 1, HEAD_DIM + 8, ch), f32),
             v((4, HEAD_DIM, ch), f32),
             v((rows + 32, 3 * ch), f32), v((group, 8, ch), f32),
-            v((2, group, length, ch), bf16), v((length, 2 * side), bf16),
-            v((length // 2, width), bf16), v((length // 2, width), bf16),
-            dma((10,)), dma((2, group - 1)), dma((2, group - 1)), dma((1,)), dma((group - 1,)), dma((2,)),
-            dma((1,)), dma((2, group - 1)), dma((1,)), dma((group,)),
-            dma((3, 2, planes)), dma((2, planes, group)), dma((planes,)),
-            dma((1,)), dma((planes, 2, group - 1)), dma((2,)), dma((4,)), dma((4,)),
-            dma((2, planes - 1)), dma((2, planes - 1)), dma((1,)), dma((2, group - 1)),
-            dma((1,)), dma((planes,)),
+            v((2, group, length, ch), bf16), v((2, length // 2, 2 * side), bf16),
+            dma((10,)), dma((1,)), dma((2, group - 1)), dma((1,)), dma((group - 1,)), dma((2,)),
+            dma((1,)), dma((5,)), dma((1,)), dma((group,)),
+            dma((3, 2)), dma((2, planes - 1, group)), dma((planes - 1,)),
+            dma((1,)), dma((planes, 3)), dma((1,)), dma((5,)), dma((2,)), dma((4,)), dma((4,)),
+            dma((2, planes - 1)), dma((2, planes - 1)), dma((2,)), dma((2, group)),
         ],
         compiler_params=pltpu.CompilerParams(
             collective_id=0, has_side_effects=True, vmem_limit_bytes=50 * 2**20

time: 99.3 us -> 97 us (0.977)
  Pallas kernels: 98.2 us -> 95.4 us
    pallas_call x1, Pallas kernels: 98.2 us -> 95.4 us  [mixer(): pl.pallas_call(functools.partial(mixer_kernel, planes, group), out_shape=...]
where the time goes in v3:
time: 97 us; the launch traced here: 96.3 us
  Pallas kernels  95.4 us (98%)
  local copies, waits for them, and re-layouts  0.97 us (1%)
    pallas_call x1, Pallas kernels, mixer(): pl.pallas_call(functools.partial(mixer_kernel, planes, group), out_shape=...  95.4 us

profile of v3, /device:TPU:0, one launch (start us, length us, event | category | flops | bytes accessed | tf_op | source)
XLA Modules:
  0.0 96.3 jit_solution(18258853727120909912)
XLA Ops:
  0.0 95.4 %shard_map.154 = bf16[256,2048]{1,0:T(8,128)(2,1)S(1)} custom-call(bf16[512,1024]{1,0:T(8,128)(2,1)} %tok_ref.1, bf16[128,512]{1,0:T(8,128)(2,1)} %key_w.1, bf16[128,512]{1,0:T(8,128)(2,1)} %query_w.1, bf16[128,512]{1,0:T(8,128)(2,1)} %value_w.1, bf16[128,512]{1,0:T(8,128)(2,1)} %gate_w.1, bf16[128,512]{1,0:T(8,128)(2,1)} %inner_w.1, ...), custom_call_target="tpu_custom_call" | custom-call | tf_op jit(solution)/shard_map/pallas_call | solution.py:1067
  95.4 1.0 %copy.18 = bf16[256,2048]{1,0:T(8,128)(2,1)} copy(bf16[256,2048]{1,0:T(8,128)(2,1)S(1)} %shard_map.154) | data formatting | bytes 2097152

commit v4 on v3

--- a/solution.py
+++ b/solution.py
@@ -761,8 +761,11 @@
         folded = passed[0:HEAD_DIM, :]
         for h in range(1, heads):
             folded = folded + passed[h * HEAD_DIM : (h + 1) * HEAD_DIM, :]
-        pack_out[target, 0:HEAD_DIM, :] = folded
-        pack_out[target, HEAD_DIM : HEAD_DIM + 8, :] = jnp.broadcast_to(over, (8, ch))
+        high = over.astype(bf16).astype(f32)
+        coefficient = jnp.where(
+            lax.broadcasted_iota(jnp.int32, (16, ch), 0) < 8, high, over - high
+        )
+        pack_out[target] = jnp.concatenate([folded, coefficient], axis=0).astype(bf16)
         return inside, reach
 
     ahead_in, ahead_reach = scan_states(state_f, ef, length - 1, range(group), 0)
@@ -826,6 +829,7 @@
     mate_copy(part_at(0), 0).start()
     arrive(CLASS_OUT, 3, ends)
     spread_out(3)
+    mate_copy(out_block(3, 0), 4).start()
     incoming = []
     for way in range(2):
         into[way] = jnp.zeros((HEAD_DIM, ch), f32)
@@ -834,10 +838,11 @@
             @pl.when(takes(way, k))
             def _(way=way, k=k):
                 pack_move(way, k).wait_recv()
-                into[way] = into[way] + into[way + 2] * pack_in[way, k - 1, 0:HEAD_DIM, :]
-                into[way + 2] = into[way + 2] * pack_in[
-                    way, k - 1, HEAD_DIM : HEAD_DIM + 1, :
-                ]
+                pack = pack_in[way, k - 1].astype(f32)
+                into[way] = into[way] + into[way + 2] * pack[0:HEAD_DIM, :]
+                into[way + 2] = into[way + 2] * (
+                    pack[HEAD_DIM : HEAD_DIM + 1, :] + pack[HEAD_DIM + 8 : HEAD_DIM + 9, :]
+                )
         incoming.append(
             jnp.where(same_head, jnp.concatenate([into[way]] * heads, axis=0), 0.0)
         )
@@ -900,6 +905,11 @@
     finish_out(1)
     for d in range(group - 1):
         mate_copy(out_block(1, d), 1).start()
+
+    def hand_over(r):
+        finish_out(r)
+        mate_copy(part_at(r), r + 1).start()
+
     arrive(CLASS_B, 3, ends)
 
     spans_at = [s * length - halo_rows for s in range(1, group)] + [all_rows]
@@ -927,8 +937,7 @@
 
     @pl.loop(0, group)
     def _(i):
-        turned_round = lax.div(i, 2)
-        d = (1 - turned_round) * (1 + 2 * i) + turned_round * (6 - 2 * i)
+        d = 3 - 2 * i + 3 * lax.div(i, 2)
         s = place_at(d)
         rows = span_rows(s)
         held = acc[rows, :] + jnp.dot(
@@ -950,6 +959,8 @@
             for c in range(2):
                 feature_move(0, d, s, c).start()
 
+        pl.when(jnp.logical_and(i == 1, ends))(lambda: hand_over(2))
+
     own_features(0)
 
     def features_here(kind, places):
@@ -978,23 +989,19 @@
     features_here(1, range(group))
     mate_here(part_at(0), 0)
     retention_product(0)
-    finish_out(2)
-    mate_copy(part_at(2), 3).start()
+    pl.when(middle)(lambda: hand_over(2))
     finish_out(3)
-    mate_copy(part_at(3), 4).start()
+    for d in range(1, group):
+        mate_copy(out_block(3, d), 4).start()
     mate_here(part_at(2), 3)
     retention_product(2)
     pair_block(source_plane(1)).wait_recv()
     mate_copy(out_block(1, 3), 2).start()
     mate_here(part_at(3), 4)
     retention_product(3)
-    features_here(0, (0, 1))
-    for r in (0, 2, 3):
-        decay[r, 0, 0:my_rows, :] = conv_product(r, own_pair)
     mate_here(pl.ds(0, (group - 1) * out_cols), 1)
     mate_here(out_block(1, 3), 2)
     retention_product(1)
-    decay[1, 0, 0:my_rows, :] = conv_product(1, own_pair)
 
     for copy in rate_moves:
         copy.wait_send()
@@ -1031,7 +1038,10 @@
 
     features_here(0, (2, 3))
     for r in range(planes):
-        out_ref[:, part_at(r)] = conv_product(r, 1 - own_pair).astype(bf16)
+        decay[r, 0, 0:my_rows, :] = conv_product(r, 1 - own_pair)
+    features_here(0, (0, 1))
+    for r in range(planes):
+        out_ref[:, part_at(r)] = conv_product(r, own_pair).astype(bf16)
     sent(parts.at[:, pl.ds(0, group - 1)], ft_send.at[0], ft_recv.at[0, 0])
     sent(parts.at[:, 0, pl.ds(0, my_rows)], ft_send.at[1], ft_recv.at[0, 0])
 
@@ -1081,7 +1091,7 @@
             table, table, table, table,
             v((group, length, ch), bf16), v((group, length, ch), bf16), v((group, length, ch), bf16),
             table, v((group, ch, ch), f32), v((group, ch, ch), f32),
-            v((2, HEAD_DIM + 8, ch), f32), v((2, planes - 1, HEAD_DIM + 8, ch), f32),
+            v((2, HEAD_DIM + 16, ch), bf16), v((2, planes - 1, HEAD_DIM + 16, ch), bf16),
             v((4, HEAD_DIM, ch), f32),
             v((rows + 32, 3 * ch), f32), v((group, 8, ch), f32),
             v((2, group, length, ch), bf16), v((2, length // 2, 2 * side), bf16),

time: 97 us -> 96.3 us (level)
  no operation moved by 1% of the time
where the time goes in v4:
time: 96.3 us; the launch traced here: 96 us
  Pallas kernels  95 us (99%)
  local copies, waits for them, and re-layouts  0.97 us (1%)
    pallas_call x1, Pallas kernels, mixer(): pl.pallas_call(functools.partial(mixer_kernel, planes, group), out_shape=...  95 us

profile of v4, /device:TPU:0, one launch (start us, length us, event | category | flops | bytes accessed | tf_op | source)
XLA Modules:
  0.0 96.0 jit_solution(8731877894834660131)
XLA Ops:
  0.0 95.0 %shard_map.154 = bf16[256,2048]{1,0:T(8,128)(2,1)S(1)} custom-call(bf16[512,1024]{1,0:T(8,128)(2,1)} %tok_ref.1, bf16[128,512]{1,0:T(8,128)(2,1)} %key_w.1, bf16[128,512]{1,0:T(8,128)(2,1)} %query_w.1, bf16[128,512]{1,0:T(8,128)(2,1)} %value_w.1, bf16[128,512]{1,0:T(8,128)(2,1)} %gate_w.1, bf16[128,512]{1,0:T(8,128)(2,1)} %inner_w.1, ...), custom_call_target="tpu_custom_call" | custom-call | tf_op jit(solution)/shard_map/pallas_call | solution.py:1077
  95.0 1.0 %copy.18 = bf16[256,2048]{1,0:T(8,128)(2,1)} copy(bf16[256,2048]{1,0:T(8,128)(2,1)S(1)} %shard_map.154) | data formatting | bytes 2097152

commit v5 on v4

--- a/solution.py
+++ b/solution.py
@@ -979,13 +979,6 @@
     def retention_product(r):
         decay[r, 0, 0:my_rows, :] = product(pl.ds(side_rows, side_rows), r)
 
-    pair_rows = 2 * ch
-    own_pair = lax.div(place, 2)
-
-    def conv_product(r, pair):
-        at = pl.ds(pl.multiple_of(pair * pair_rows, 128), pair_rows)
-        return decay[r, 0, 0:my_rows, :] + product(at, r)
-
     features_here(1, range(group))
     mate_here(part_at(0), 0)
     retention_product(0)
@@ -1036,12 +1029,11 @@
             pl.when(plane == units - 1)(functools.partial(far_sent, kind, 0, units))
             pl.when(plane == planes - units)(functools.partial(far_sent, kind, 1, units))
 
-    features_here(0, (2, 3))
+    features_here(0, (0, 1, 2, 3))
     for r in range(planes):
-        decay[r, 0, 0:my_rows, :] = conv_product(r, 1 - own_pair)
-    features_here(0, (0, 1))
-    for r in range(planes):
-        out_ref[:, part_at(r)] = conv_product(r, own_pair).astype(bf16)
+        out_ref[:, part_at(r)] = (
+            decay[r, 0, 0:my_rows, :] + product(pl.ds(0, side_rows), r)
+        ).astype(bf16)
     sent(parts.at[:, pl.ds(0, group - 1)], ft_send.at[0], ft_recv.at[0, 0])
     sent(parts.at[:, 0, pl.ds(0, my_rows)], ft_send.at[1], ft_recv.at[0, 0])
 

time: 96.3 us -> 96.3 us (level)
  no operation moved by 1% of the time
where the time goes in v5:
time: 96.3 us; the launch traced here: 95.9 us
  Pallas kernels  94.9 us (99%)
  local copies, waits for them, and re-layouts  0.97 us (1%)
    pallas_call x1, Pallas kernels, mixer(): pl.pallas_call(functools.partial(mixer_kernel, planes, group), out_shape=...  94.9 us

profile of v5, /device:TPU:0, one launch (start us, length us, event | category | flops | bytes accessed | tf_op | source)
XLA Modules:
  0.0 95.9 jit_solution(5787642899077327266)
XLA Ops:
  0.0 94.9 %shard_map.154 = bf16[256,2048]{1,0:T(8,128)(2,1)S(1)} custom-call(bf16[512,1024]{1,0:T(8,128)(2,1)} %tok_ref.1, bf16[128,512]{1,0:T(8,128)(2,1)} %key_w.1, bf16[128,512]{1,0:T(8,128)(2,1)} %query_w.1, bf16[128,512]{1,0:T(8,128)(2,1)} %value_w.1, bf16[128,512]{1,0:T(8,128)(2,1)} %gate_w.1, bf16[128,512]{1,0:T(8,128)(2,1)} %inner_w.1, ...), custom_call_target="tpu_custom_call" | custom-call | tf_op jit(solution)/shard_map/pallas_call | solution.py:1069
  94.9 1.0 %copy.18 = bf16[256,2048]{1,0:T(8,128)(2,1)} copy(bf16[256,2048]{1,0:T(8,128)(2,1)S(1)} %shard_map.154) | data formatting | bytes 2097152
